TPU v7x, 256 devices: a whole 4x4x8 slice. The times are simulated.
256 devices in a mesh: sp: 64 (over z, x, core), tp: 4 (over y).
Axes of the slice: x: 4, y: 4, z: 8, core: 2. Of those that a mesh axis runs over, the one named last changes fastest.
Arguments:
- conv_out: bfloat16 [12288, 2048], P('sp', 'tp'), may hold values from -6 to 6
- gate_in: bfloat16 [12288, 2048], P('sp', 'tp'), may hold values from -6 to 6
- block_states: float32 [64, 2048], P('sp', 'tp'), may hold values from -4 to 4
- decay_param: float32 [2048], P('tp'), may hold values from 4 to 20
- decay_shift: float32 [12288], P('sp'), may hold values from -2 to 0, as said below
- w_reset: bfloat16 [16, 128, 128], P('tp'), may hold values from -0.5 to 0.5
- w_input: bfloat16 [16, 128, 128], P('tp'), may hold values from -0.5 to 0.5
- w_out: bfloat16 [2048, 2048], P('tp'), may hold values from -0.125 to 0.125
- mixed: bfloat16 [12288, 2048], P('sp', 'tp'), may hold values from -6 to 6
- d_out: bfloat16 [12288, 2048], P('sp', 'tp'), may hold values from -16 to 16
- expert_ids: int32 [12288, 2], P('sp'), may hold values from 0 to 63, all different within a row; in each aligned block of 192 rows (0 to 191, 192 to 383, ...) at most 12 rows name the same one
- route_weights: float32 [12288, 2], P('sp'), may hold values from 0.2 to 1.4
- w_gate: bfloat16 [64, 2048, 1024], P('sp', None, 'tp'), may hold values from -0.125 to 0.125
- w_up: bfloat16 [64, 2048, 1024], P('sp', None, 'tp'), may hold values from -0.125 to 0.125
- w_down: bfloat16 [64, 1024, 2048], P('sp', 'tp'), may hold values from -0.1875 to 0.1875
Outputs:
- grad_w_gate: float32 [64, 2048, 1024], P('sp', None, 'tp')
- grad_w_up: float32 [64, 2048, 1024], P('sp', None, 'tp')
- grad_w_down: float32 [64, 1024, 2048], P('sp', 'tp')
- grad_out_proj_t: float32 [2048, 2048], P('sp', 'tp')
- recurrence_input_gradient: bfloat16 [12288, 2048], P('sp', 'tp')
- grad_gate: bfloat16 [12288, 2048], P('sp', 'tp')
Inputs may be any that keep to these rules, and one draw needn't show every extreme that they name: `expert_ids`: each row names 2 different experts; among the 192 tokens of one index of sp no expert is named more than 12 times, and in some index of sp one expert is named exactly 12 times. decay_shift is at most -0.05 / 12288 at every position.
All inputs are finite; a program needn't handle non-finite values.
Results may differ from a plain program's by a relative error of at most 0.013.
Values may be sent and summed in bfloat16 or wider, within the bound.
A program may use at most 128 MiB of HBM per device.

v0:
```python
import jax
import jax.numpy as jnp
from jax import lax
from jax.sharding import Mesh
from jax.sharding import PartitionSpec as P

SP = ("sp_0", "sp_1", "sp_2")


def in_one_piece(arrays, axis, split_dim, concat_dim, along):
    widths = [a.shape[along] for a in arrays]
    both = jnp.concatenate(arrays, axis=along)
    filled = lax.all_to_all(both, axis, split_axis=split_dim, concat_axis=concat_dim, tiled=True)
    return tuple(jnp.split(filled, [sum(widths[:k]) for k in range(1, len(widths))], axis=along))


def side_by_side(arrays, axis, dim, along):
    both = jnp.concatenate(arrays, axis=along)
    filled, at, done = (lax.all_gather(both, axis, axis=dim, tiled=True), 0, [])
    for a in arrays:
        done.append(lax.slice_in_dim(filled, at, at + a.shape[along], axis=along))
        at += a.shape[along]
    return tuple(done)


def split_up(value, dim, devices):
    before, after = (value.shape[:dim], value.shape[dim + 1 :])
    return jnp.moveaxis(value.reshape(*before, devices, -1, *after), dim, 0)


def sent_and_summed(value, axis, dim):
    devices = lax.axis_size(axis)
    parts = lax.all_to_all(split_up(value, dim, devices), axis, 0, 0, tiled=True)
    return jnp.sum(parts.astype(jnp.float32), axis=0)


def copy_for_each(value, axis):
    devices = lax.axis_size(axis)
    return lax.all_to_all(
        jnp.broadcast_to(value[None], (devices, *value.shape)), axis, 0, 0, tiled=True
    )


def in_order(parts, dim):
    parts = jnp.moveaxis(parts, 0, dim)
    lengths = parts.shape
    return parts.reshape(*lengths[:dim], lengths[dim] * lengths[dim + 1], *lengths[dim + 2 :])


def collect(value, axis, dim):
    parts = copy_for_each(value, axis)
    return in_order(parts, dim)


def own_rows(terms, axes):
    so_far = terms.astype(jnp.bfloat16)
    for axis in axes:
        so_far = lax.psum_scatter(so_far, axis, scatter_dimension=0, tiled=True)
    return so_far.astype(jnp.float32)


def all_in_one(value, axis):
    leaves = jax.tree.leaves(value)
    turns = sorted(range(len(leaves)), key=lambda k: -leaves[k].size)
    width = (1, *leaves[turns[0]].shape)[-1]
    lines = [
        jnp.pad(leaves[k].reshape(-1), (0, -leaves[k].size % width)).reshape(-1, width)
        for k in turns
    ]
    both, at, found = (copy_for_each(jnp.concatenate(lines), axis), 0, {})
    for k, line in zip(turns, lines):
        section = both[:, at : at + len(line)].reshape(len(both), -1)
        found[k] = section[:, : leaves[k].size].reshape(-1, *leaves[k].shape)
        at += len(line)
    numbers = iter(range(len(leaves)))
    return jax.tree.map(lambda _: found[next(numbers)], value)


def combined_pairwise(pieces, combine):
    while len(jax.tree.leaves(pieces)[0]) > 1:
        pieces = jax.vmap(combine)(
            *(jax.tree.map(lambda part: part[side::2], pieces) for side in (0, 1))
        )
    return jax.tree.map(lambda part: part[0], pieces)


def entering(value, axis, combine, identity):
    devices, here = (lax.axis_size(axis), lax.axis_index(axis))
    passed = jnp.arange(devices) > here

    def kept(part, zero, own):
        part = jnp.where(
            passed.reshape(-1, *(1 for _ in own.shape)), part, jnp.asarray(zero, own.dtype)
        )
        return part[::-1]

    pieces = all_in_one(value, axis)
    return combined_pairwise(jax.tree.map(kept, pieces, identity, value), combine)


def decay_combine(first_pair, second_pair):
    return (first_pair[0] * second_pair[0], second_pair[0] * first_pair[1] + second_pair[1])


def carry_combine(earlier_pair, later_pair):
    return (later_pair[0] * earlier_pair[0], later_pair[1] + later_pair[0] * earlier_pair[1])


def gelu_slope(values):
    outcome, pullback = jax.vjp(jax.nn.gelu, values)
    return (outcome, pullback(jnp.ones_like(values))[0])


def head_maps(values, weights):
    count = values.shape[0]
    split = values.reshape(count, weights.shape[0], weights.shape[1])
    mapped = jnp.einsum("thi,hij->thj", split, weights, preferred_element_type=jnp.float32)
    return mapped.reshape(count, -1)


def head_back(grads, weights):
    count = grads.shape[0]
    split = grads.reshape(count, weights.shape[0], weights.shape[2])
    mapped = jnp.einsum("thj,hij->thi", split, weights, preferred_element_type=jnp.float32)
    return mapped.reshape(count, -1)


def over_rows(left_matrix, right_matrix):
    return lax.dot_general(
        left_matrix, right_matrix, (((0,), (0,)), ((), ())), preferred_element_type=jnp.float32
    )


def against_rows(left_matrix, right_matrix):
    return lax.dot_general(
        left_matrix, right_matrix, (((1,), (1,)), ((), ())), preferred_element_type=jnp.float32
    )


def slot_layout(expert_ids, experts, capacity):
    tok_rows, top_k = expert_ids.shape
    flat_ids = expert_ids.reshape(-1)
    onehot = (flat_ids[:, None] == jnp.arange(experts, dtype=jnp.int32)[None, :]).astype(jnp.int32)
    slot_rank = jnp.sum((jnp.cumsum(onehot, axis=0) - 1) * onehot, axis=1)
    slot_index = flat_ids * capacity + slot_rank
    slot_table = (
        jnp.full((experts * capacity,), tok_rows * top_k, jnp.int32)
        .at[slot_index]
        .set(jnp.arange(tok_rows * top_k, dtype=jnp.int32))
    )
    return (slot_index, slot_table)


def place_slots(cot_part, row_part, route_weights, slot_table, experts, capacity):
    tok_rows, top_k = route_weights.shape
    columns = cot_part.shape[1]
    scaled = (
        (route_weights[:, :, None] * cot_part.astype(jnp.float32)[:, None, :])
        .astype(jnp.bfloat16)
        .reshape(tok_rows * top_k, columns)
    )
    scaled = jnp.concatenate([scaled, jnp.zeros((1, columns), jnp.bfloat16)], axis=0)
    padded = jnp.concatenate([row_part, jnp.zeros((1, columns), jnp.bfloat16)], axis=0)
    token_ids = jnp.where(slot_table < tok_rows * top_k, slot_table // top_k, tok_rows)
    send_cot = scaled[slot_table].reshape(experts, capacity, columns)
    send_rows = padded[token_ids].reshape(experts, capacity, columns)
    return (send_cot, send_rows)


def expert_terms(expert_in, expert_cot, gate_matrix, up_matrix, down_matrix):
    up_pre = jnp.dot(expert_in, gate_matrix, preferred_element_type=jnp.float32)
    linear = jnp.dot(expert_in, up_matrix, preferred_element_type=jnp.float32)
    sigmoid_up = jax.nn.sigmoid(up_pre)
    silu_up = up_pre * sigmoid_up
    hidden_state = (silu_up * linear).astype(jnp.bfloat16)
    d_hidden = against_rows(expert_cot, down_matrix)
    d_linear = (d_hidden * silu_up).astype(jnp.bfloat16)
    d_up = (d_hidden * linear * sigmoid_up * (1.0 + up_pre * (1.0 - sigmoid_up))).astype(
        jnp.bfloat16
    )
    grad_gate_e = over_rows(expert_in, d_up)
    grad_up_e = over_rows(expert_in, d_linear)
    grad_down_e = over_rows(hidden_state, expert_cot)
    partial_value = against_rows(d_up, gate_matrix) + against_rows(d_linear, up_matrix)
    return (grad_gate_e, grad_up_e, grad_down_e, partial_value)


def body(
    conv_out,
    gate_in,
    block_states,
    decay_param,
    decay_shift,
    w_reset,
    w_input,
    w_out,
    mixed,
    d_out,
    expert_ids,
    route_weights,
    w_gate,
    w_up,
    w_down,
):
    tok_rows, top_k = expert_ids.shape
    experts = lax.axis_size(SP)
    capacity = 2 * tok_rows * top_k // experts
    conv_full = conv_out.astype(jnp.float32)
    reset = jax.nn.sigmoid(head_maps(conv_out, w_reset))
    input_gate = jax.nn.sigmoid(head_maps(conv_out, w_input))
    slow_rate = jax.nn.softplus(-decay_param)
    log_decay = -8.0 * reset * slow_rate[None, :] + decay_shift[:, None]
    decays = jnp.exp(log_decay)
    norm_in = jnp.sqrt(-jnp.expm1(2.0 * log_decay))
    drives = norm_in * input_gate * conv_full
    cum_decay, cum_drive = lax.associative_scan(decay_combine, (decays, drives), axis=0)
    states = cum_decay * block_states + cum_drive
    prev_states = jnp.concatenate([block_states, states[:-1]], axis=0)
    gate_act, gate_deriv = gelu_slope(gate_in.astype(jnp.float32))
    merged_in = (gate_act * states).astype(jnp.bfloat16)
    slot_index, slot_table = slot_layout(expert_ids, experts, capacity)
    send_cot, send_rows = place_slots(d_out, mixed, route_weights, slot_table, experts, capacity)
    part_cot, part_rows = in_one_piece((send_cot, send_rows), SP, 0, 0, 1)
    got_cot, got_rows = side_by_side((part_cot, part_rows), "tp", 2, 0)
    width_full = got_cot.shape[2]
    grad_gate_e, grad_up_e, grad_down_e, partial_value = expert_terms(
        got_rows.reshape(-1, width_full),
        got_cot.reshape(-1, width_full),
        w_gate[0],
        w_up[0],
        w_down[0],
    )
    row_grad = sent_and_summed(partial_value.astype(jnp.bfloat16), "tp", 1).astype(jnp.bfloat16)
    columns = row_grad.shape[1]
    returned = lax.all_to_all(
        row_grad.reshape(experts, capacity, columns), SP, split_axis=0, concat_axis=0, tiled=True
    )
    summed = jnp.sum(
        returned.reshape(-1, columns)[slot_index]
        .astype(jnp.float32)
        .reshape(tok_rows, top_k, columns),
        axis=1,
    )
    d_columns = (d_out.astype(jnp.float32) + summed).astype(jnp.bfloat16)
    d_mixed = collect(d_columns, "tp", 1)
    grad_out_proj_t = own_rows(over_rows(d_mixed, merged_in), SP)
    d_merged = against_rows(d_mixed, w_out)
    grad_gate = (d_merged * states * gate_deriv).astype(jnp.bfloat16)
    d_states = d_merged * gate_act
    next_decay = jnp.concatenate([decays[1:], jnp.ones((1, decays.shape[1]), jnp.float32)], axis=0)
    prods_flipped, local_flipped = lax.associative_scan(
        decay_combine, (next_decay[::-1], d_states[::-1]), axis=0
    )
    products = prods_flipped[::-1]
    local_grad = local_flipped[::-1]
    block_prod = products[0] * decays[0]
    block_lead = decays[0] * local_grad[0]
    incoming = entering(
        (block_prod, block_lead),
        SP,
        carry_combine,
        (jnp.ones_like(block_prod), jnp.zeros_like(block_lead)),
    )
    state_grad = local_grad + products * incoming[1][None, :]
    d_log_decay = (
        state_grad * decays * prev_states
        - state_grad * input_gate * conv_full * decays * decays / norm_in
    )
    d_pre_reset = (d_log_decay * (-8.0 * slow_rate[None, :]) * reset * (1.0 - reset)).astype(
        jnp.bfloat16
    )
    d_pre_input = (state_grad * norm_in * conv_full * input_gate * (1.0 - input_gate)).astype(
        jnp.bfloat16
    )
    recurrence_input_gradient = (
        state_grad * norm_in * input_gate
        + head_back(d_pre_reset, w_reset)
        + head_back(d_pre_input, w_input)
    ).astype(jnp.bfloat16)
    return (
        grad_gate_e[None],
        grad_up_e[None],
        grad_down_e[None],
        grad_out_proj_t,
        recurrence_input_gradient,
        grad_gate,
    )


def solution(mesh):
    torus = Mesh(mesh.devices.reshape(8, 4, 2, mesh.shape["tp"]), ("sp_0", "sp_1", "sp_2", "tp"))
    in_specs = (
        P(SP, "tp"),
        P(SP, "tp"),
        P(SP, "tp"),
        P("tp"),
        P(SP),
        P("tp", None, None),
        P("tp", None, None),
        P("tp", None),
        P(SP, "tp"),
        P(SP, "tp"),
        P(SP, None),
        P(SP, None),
        P(SP, None, "tp"),
        P(SP, None, "tp"),
        P(SP, "tp", None),
    )
    out_specs = (
        P(SP, None, "tp"),
        P(SP, None, "tp"),
        P(SP, "tp", None),
        P(SP, "tp"),
        P(SP, "tp"),
        P(SP, "tp"),
    )
    return jax.shard_map(body, mesh=torus, in_specs=in_specs, out_specs=out_specs, check_vma=False)
```

profile of v0, /device:TPU:16, one launch (start us, length us, event | category | flops | bytes accessed | tf_op | source)
XLA Modules:
  0.0 500.7 jit_solution(14403873241260485137)
XLA Ops:
  10.8 2.9 scatter_custom_fusion
  14.7 3.3 gather_fusion.1
  20.4 2.6 mul.421
  24.5 3.3 gather_fusion
  31.7 51.8 %all_to_all.25 = bf16[64,24,512]{2,1,0:T(8,128)(2,1)S(1)} all-to-all(bf16[64,24,512]{2,1,0:T(8,128)(2,1)S(1)} %pad_maximum_fusion.1), channel_id=1, replica_groups=mesh['sp_0'=8,'sp_1'=4,'sp_2'=2,'tp'=4] {'sp_0','sp_1','sp_2'}, dimensions={0} | all-to-all | bytes 3145728 | tf_op jit(solution)/shard_map/all_to_all | solution.py:13
  99.2 68.1 %all-gather.2.cloned.1.call-done = bf16[128,12,2048]{2,1,0:T(8,128)(2,1)} async-done(((bf16[128,12,512]{2,1,0:T(8,128)(2,1)}), bf16[128,12,2048]{2,1,0:T(8,128)(2,1)}) %all-gather.2.cloned.1.call-update) | async-done | bytes 6291472 | tf_op jit(solution)/shard_map/all_gather | solution.py:19
  167.3 6.1 %fusion.94 = (bf16[64,12,2048]{2,1,0:T(8,128)(2,1)}, bf16[64,12,2048]{2,1,0:T(8,128)(2,1)}) fusion(bf16[128,12,2048]{2,1,0:T(8,128)(2,1)} %all-gather.2.cloned.1.call-done), kind=kLoop, calls=%fused_computation.242 | loop fusion | bytes 12582912 | tf_op jit(solution)/shard_map/slice | solution.py:21
  173.5 6.2 %reshape.147 = bf16[768,2048]{1,0:T(8,128)(2,1)} reshape(bf16[64,12,2048]{2,1,0:T(8,128)(2,1)} %get-tuple-element.19) | data formatting | bytes 6291456 | tf_op jit(solution)/shard_map/reshape | solution.py:227
  179.6 4.2 fusion.10
  185.7 6.1 %reshape.148 = bf16[768,2048]{1,0:T(8,128)(2,1)} reshape(bf16[64,12,2048]{2,1,0:T(8,128)(2,1)} %get-tuple-element.18) | data formatting | bytes 6291456 | tf_op jit(solution)/shard_map/reshape | solution.py:228
  191.9 3.9 multiply_convert_fusion.1
  200.3 5.6 %all-to-all-start.1 = ((bf16[4,768,512]{2,1,0:T(8,128)(2,1)}), bf16[4,768,512]{2,1,0:T(8,128)(2,1)}, u32[]{:S(2)}, u32[]{:S(2)}) async-start(bf16[4,768,512]{2,1,0:T(8,128)(2,1)} %bitcast.160), calls=%async_computation.1 | async-start | bytes 6291456 | tf_op jit(solution)/shard_map/all_to_all | solution.py:33
  207.9 32.9 %all-to-all-done.1 = bf16[4,768,512]{2,1,0:T(8,128)(2,1)} async-done(((bf16[4,768,512]{2,1,0:T(8,128)(2,1)}), bf16[4,768,512]{2,1,0:T(8,128)(2,1)}, u32[]{:S(2)}, u32[]{:S(2)}) %all-to-all-start.1) | async-done | bytes 3145760 | tf_op jit(solution)/shard_map/all_to_all | solution.py:33
  240.8 2.8 reduce_sum.34
  244.8 11.1 %all-to-all-start.2 = ((bf16[64,12,512]{2,1,0:T(8,128)(2,1)}), bf16[64,12,512]{2,1,0:T(8,128)(2,1)}, u32[]{:S(2)}, u32[]{:S(2)}) async-start(bf16[64,12,512]{2,1,0:T(8,128)(2,1)} %reshape.150), calls=%async_computation.2 | async-start | bytes 2097152 | tf_op jit(solution)/shard_map/all_to_all | solution.py:235
  291.8 2.5 pad.203
  295.6 2.6 gather_fusion.2
  303.5 6.4 %all-to-all-start.3 = ((bf16[4,192,512]{2,1,0:T(8,128)(2,1)}), bf16[4,192,512]{2,1,0:T(8,128)(2,1)S(1)}, u32[]{:S(2)}, u32[]{:S(2)}) async-start(bf16[4,192,512]{2,1,0:T(8,128)(2,1)} %broadcast_in_dim.66), calls=%async_computation.3 | async-start | bytes 1572864 | tf_op jit(solution)/shard_map/all_to_all | solution.py:39
  313.1 2.5 pad.189
  315.6 2.9 slice.621
  318.5 2.8 slice.630
  321.3 2.8 slice.623
  324.8 4.3 convolution_bitcast_fusion.2
  331.2 3.4 fusion.22
  337.3 2.8 slice.627
  398.8 3.3 convolution_convert_fusion
  426.4 10.0 %all-to-all-start.4 = ((f32[64,2,512]{2,1,0:T(2,128)}), f32[64,2,512]{2,1,0:T(2,128)S(1)}, u32[]{:S(2)}, u32[]{:S(2)}) async-start(f32[64,2,512]{2,1,0:T(2,128)} %broadcast_in_dim.68), calls=%async_computation.7 | async-start | bytes 524288 | tf_op jit(solution)/shard_map/all_to_all | solution.py:39
  436.8 4.5 convolution_bitcast_fusion.1
  444.6 2.7 rev.4
  447.3 4.5 rev.5
  457.3 20.5 %reduce-scatter.6.cloned.1.call-done = bf16[64,512]{1,0:T(8,128)(2,1)} async-done(((bf16[256,512]{1,0:T(8,128)(2,1)}), bf16[64,512]{1,0:T(8,128)(2,1)}) %reduce-scatter.6.cloned.1.call-update) | async-done | bytes 65552 | tf_op jit(solution)/shard_map/reduce_scatter | solution.py:58
  479.6 13.2 %reduce-scatter.8.cloned.1.call-done = bf16[32,512]{1,0:T(8,128)(2,1)} async-done(((bf16[64,512]{1,0:T(8,128)(2,1)}), bf16[32,512]{1,0:T(8,128)(2,1)}) %reduce-scatter.8.cloned.1.call-update) | async-done | bytes 32784 | tf_op jit(solution)/shard_map/reduce_scatter | solution.py:58
  (453 shorter events, 182.6 us)
Async XLA Ops:
  7.2 324.0 %copy-start = (bf16[512,2048]{1,0:T(8,128)(2,1)S(1)}, bf16[512,2048]{1,0:T(8,128)(2,1)}, u32[]{:S(2)}) copy-start(bf16[512,2048]{1,0:T(8,128)(2,1)} %param.22) | copy-start | bytes 6291460
  7.2 160.1 %all-gather.2.cloned.1.call-start = ((), (), s32[]{:S(2)}) async-start(), calls=%async_computation.8 | async-start | bytes 10485760 | tf_op jit(solution)/shard_map/all_gather | solution.py:19
  87.7 85.8 %copy-start.6 = (f32[192,512]{1,0:T(8,128)}, f32[192,512]{1,0:T(8,128)S(1)}, u32[]{:S(2)}) copy-start(f32[192,512]{1,0:T(8,128)S(1)} %get-tuple-element.27) | copy-start | bytes 1179652
  96.9 76.5 %copy-start.23 = (f32[48,512]{1,0:T(8,128)}, f32[48,512]{1,0:T(8,128)S(1)}, u32[]{:S(2)}) copy-start(f32[48,512]{1,0:T(8,128)S(1)} %get-tuple-element.47) | copy-start | bytes 294916
  97.0 76.5 %copy-start.24 = (f32[48,512]{1,0:T(8,128)}, f32[48,512]{1,0:T(8,128)S(1)}, u32[]{:S(2)}) copy-start(f32[48,512]{1,0:T(8,128)S(1)} %get-tuple-element.46) | copy-start | bytes 294916
  200.3 40.5 %all-to-all-start.1 = ((bf16[4,768,512]{2,1,0:T(8,128)(2,1)}), bf16[4,768,512]{2,1,0:T(8,128)(2,1)}, u32[]{:S(2)}, u32[]{:S(2)}) async-start(bf16[4,768,512]{2,1,0:T(8,128)(2,1)} %bitcast.160), calls=%async_computation.1 | async-start | bytes 6291456 | tf_op jit(solution)/shard_map/all_to_all | solution.py:33
  244.8 25.8 %copy-start.7 = (f32[192,512]{1,0:T(8,128)S(1)}, f32[192,512]{1,0:T(8,128)}, u32[]{:S(2)}) copy-start(f32[192,512]{1,0:T(8,128)} %copy-done.6) | copy-start | bytes 1179652
  244.8 49.5 %all-to-all-start.2 = ((bf16[64,12,512]{2,1,0:T(8,128)(2,1)}), bf16[64,12,512]{2,1,0:T(8,128)(2,1)}, u32[]{:S(2)}, u32[]{:S(2)}) async-start(bf16[64,12,512]{2,1,0:T(8,128)(2,1)} %reshape.150), calls=%async_computation.2 | async-start | bytes 2097152 | tf_op jit(solution)/shard_map/all_to_all | solution.py:235
  261.0 14.5 %copy-start.35 = (f32[12,512]{1,0:T(8,128)S(1)}, f32[12,512]{1,0:T(8,128)}, u32[]{:S(2)}) copy-start(f32[12,512]{1,0:T(8,128)} %add.431) | copy-start | bytes 73732
  264.5 14.0 %copy-start.34 = (f32[23,512]{1,0:T(8,128)S(1)}, f32[23,512]{1,0:T(8,128)}, u32[]{:S(2)}) copy-start(f32[23,512]{1,0:T(8,128)} %slice.580) | copy-start | bytes 141316
  273.2 9.0 %copy-start.25 = (f32[47,512]{1,0:T(8,128)S(1)}, f32[47,512]{1,0:T(8,128)}, u32[]{:S(2)}) copy-start(f32[47,512]{1,0:T(8,128)} %slice.582) | copy-start | bytes 288772
  273.2 9.0 %copy-start.26 = (f32[47,512]{1,0:T(8,128)S(1)}, f32[47,512]{1,0:T(8,128)}, u32[]{:S(2)}) copy-start(f32[47,512]{1,0:T(8,128)} %slice.615) | copy-start | bytes 288772
  274.8 13.7 %copy-start.17 = (f32[95,512]{1,0:T(8,128)S(1)}, f32[95,512]{1,0:T(8,128)}, u32[]{:S(2)}) copy-start(f32[95,512]{1,0:T(8,128)} %slice.584) | copy-start | bytes 583684
  280.0 10.2 %copy-start.50 = (f32[1,512]{1,0:T(1,128)S(1)}, f32[1,512]{1,0:T(1,128)}, u32[]{:S(2)}) copy-start(f32[1,512]{1,0:T(1,128)} %slice.752) | copy-start | bytes 6148
  282.2 12.1 %copy-start.57 = (s32[384]{0:T(512)S(1)}, s32[384]{0:T(512)}, u32[]{:S(2)}) copy-start(s32[384]{0:T(512)} %copy-done.56) | copy-start | bytes 4612
  298.2 11.7 %copy-start.18 = (f32[95,512]{1,0:T(8,128)S(1)}, f32[95,512]{1,0:T(8,128)}, u32[]{:S(2)}) copy-start(f32[95,512]{1,0:T(8,128)} %get-tuple-element.36) | copy-start | bytes 583684
  298.2 11.7 %copy-start.49 = (f32[1,512]{1,0:T(1,128)S(1)}, f32[1,512]{1,0:T(1,128)}, u32[]{:S(2)}) copy-start(f32[1,512]{1,0:T(1,128)} %slice.731) | copy-start | bytes 6148
  303.5 25.6 %all-to-all-start.3 = ((bf16[4,192,512]{2,1,0:T(8,128)(2,1)}), bf16[4,192,512]{2,1,0:T(8,128)(2,1)S(1)}, u32[]{:S(2)}, u32[]{:S(2)}) async-start(bf16[4,192,512]{2,1,0:T(8,128)(2,1)} %broadcast_in_dim.66), calls=%async_computation.3 | async-start | bytes 1572864 | tf_op jit(solution)/shard_map/all_to_all | solution.py:39
  310.0 143.2 %reduce-scatter.4.cloned.1.call-start = ((), (), s32[]{:S(2)}) async-start(), calls=%async_computation.9 | async-start | bytes 2359296 | tf_op jit(solution)/shard_map/reduce_scatter | solution.py:58
  397.0 8.3 %copy-start.43 = (f32[5,512]{1,0:T(8,128)S(1)}, f32[5,512]{1,0:T(8,128)}, u32[]{:S(2)}) copy-start(f32[5,512]{1,0:T(8,128)} %slice.668) | copy-start | bytes 30724
  402.2 8.7 %copy-start.19 = (f32[95,512]{1,0:T(8,128)S(1)}, f32[95,512]{1,0:T(8,128)}, u32[]{:S(2)}) copy-start(f32[95,512]{1,0:T(8,128)} %slice.676) | copy-start | bytes 583684
  405.5 11.5 %copy-start.16 = (f32[95,512]{1,0:T(8,128)S(1)}, f32[95,512]{1,0:T(8,128)}, u32[]{:S(2)}) copy-start(f32[95,512]{1,0:T(8,128)} %slice.621) | copy-start | bytes 583684
  406.4 12.4 %copy-start.48 = (f32[1,512]{1,0:T(1,128)S(1)}, f32[1,512]{1,0:T(1,128)}, u32[]{:S(2)}) copy-start(f32[1,512]{1,0:T(1,128)} %slice.773) | copy-start | bytes 6148
  426.4 25.4 %all-to-all-start.4 = ((f32[64,2,512]{2,1,0:T(2,128)}), f32[64,2,512]{2,1,0:T(2,128)S(1)}, u32[]{:S(2)}, u32[]{:S(2)}) async-start(f32[64,2,512]{2,1,0:T(2,128)} %broadcast_in_dim.68), calls=%async_computation.7 | async-start | bytes 524288 | tf_op jit(solution)/shard_map/all_to_all | solution.py:39
  436.4 41.4 %reduce-scatter.6.cloned.1.call-start = ((), (), s32[]{:S(2)}) async-start(), calls=%async_computation.10 | async-start | bytes 327680 | tf_op jit(solution)/shard_map/reduce_scatter | solution.py:58
  443.7 8.4 %copy-start.62 = (pred[64]{0:T(512)(128)(4,1)S(1)}, pred[64]{0:T(512)(128)(4,1)}, u32[]{:S(2)}) copy-start(pred[64]{0:T(512)(128)(4,1)} %iota_compare_fusion.2) | copy-start | bytes 196
  443.7 9.5 %copy-start.2 = (f32[4,24,8,128]{3,2,1,0:T(8,128)S(1)}, f32[4,24,8,128]{3,2,1,0:T(8,128)}, u32[]{:S(2)}) copy-start(f32[4,24,8,128]{3,2,1,0:T(8,128)} %copy-done.1) | copy-start | bytes 1179652
  443.8 9.5 %copy-start.10 = (f32[192,512]{1,0:T(8,128)S(1)}, f32[192,512]{1,0:T(8,128)}, u32[]{:S(2)}) copy-start(f32[192,512]{1,0:T(8,128)} %get-tuple-element.7) | copy-start | bytes 1179652
  443.8 9.5 %copy-start.45 = (f32[512]{0:T(512)S(1)}, f32[512]{0:T(512)}, u32[]{:S(2)}) copy-start(f32[512]{0:T(512)} %copy-done.44) | copy-start | bytes 6148
  443.8 9.5 %copy-start.47 = (f32[1,512]{1,0:T(1,128)S(1)}, f32[1,512]{1,0:T(1,128)}, u32[]{:S(2)}) copy-start(f32[1,512]{1,0:T(1,128)} %param.17) | copy-start | bytes 6148
  443.8 9.5 %copy-start.59 = (f32[192]{0:T(256)S(1)}, f32[192]{0:T(256)}, u32[]{:S(2)}) copy-start(f32[192]{0:T(256)} %param.19) | copy-start | bytes 2308
  453.2 39.6 %reduce-scatter.8.cloned.1.call-start = ((), (), s32[]{:S(2)}) async-start(), calls=%async_computation.11 | async-start | bytes 98304 | tf_op jit(solution)/shard_map/reduce_scatter | solution.py:58
  (41 other events, 149.8 us)
Sparse Core Ops, SparseCore 0:
  85.8 81.4 all-gather.1
  402.3 48.3 reduce-scatter.3
  453.3 24.4 reduce-scatter.5
  480.1 12.5 reduce-scatter.7
where the time goes:
time: 508 us; the launch traced here: 501 us
  local copies, waits for them, and re-layouts  173 us (34%)
  waiting for transfers between devices  135 us (27%)
  other arithmetic  59.6 us (12%)
  blocking collectives  51.8 us (10%)
  starting transfers between devices  33.5 us (7%)
  matrix products  32.4 us (6%)
  between operations  15.3 us (3%)
    slice x53, local copies, waits for them, and re-layouts, body(): lax.associative_scan(decay_combine, (next_decay[::-1], d_states[::-1]), a...  68.3 us
    all_gather x1, waiting for transfers between devices, side_by_side(): filled, at, done = (lax.all_gather(both, axis, axis=dim, tiled=True), 0, [])  68.1 us
    all_to_all x1, blocking collectives, in_one_piece(): lax.all_to_all(both, axis, split_axis=split_dim, concat_axis=concat_dim,...  51.8 us
    reduce_scatter x3, waiting for transfers between devices, own_rows(): so_far = lax.psum_scatter(so_far, axis, scatter_dimension=0, tiled=True)  33.7 us
    all_to_all x1, waiting for transfers between devices, sent_and_summed(): lax.all_to_all(split_up(value, dim, devices), axis, 0, 0, tiled=True)  32.9 us
    slice x48, local copies, waits for them, and re-layouts, body(): lax.associative_scan(decay_combine, (decays, drives), axis=0)  21.7 us
    mul x26, other arithmetic, decay_combine(): first_pair[0] * second_pair[0]  20.5 us
    all_to_all x2, starting transfers between devices, copy_for_each(): lax.all_to_all(jnp.broadcast_to(value[None], (devices, *value.shape)), ax...  16.5 us
  transfers between devices with their start and end apart: 8, of which 4 were waited for; matrix products, arithmetic and copies ran while one was open for 23% of the time, Pallas kernels for 0%

commit v1 on v0

v1 whole, which is shorter than its diff:
```python
import functools

import jax
import jax.numpy as jnp
from jax import lax
from jax.experimental import pallas as pl
from jax.experimental.pallas import tpu as pltpu
from jax.sharding import PartitionSpec as P

F32 = jnp.float32
BF16 = jnp.bfloat16
MESH = pl.DeviceIdType.MESH
Z_ORDER = (0, 1, 7, 2, 6, 3, 5, 4)
VM = pl.BlockSpec(memory_space=pltpu.VMEM)
ANY = pl.BlockSpec(memory_space=pl.ANY)


def dot(a, b, dims=((1,), (0,))):
    return lax.dot_general(a, b, (dims, ((), ())), preferred_element_type=F32)


def swap4(value):
    return pltpu.roll(value, 4, axis=1)


def low_half(shape):
    return lax.broadcasted_iota(jnp.int32, shape, 1) < 4


def forward_kernel(
    conv_ref, gate_ref, first_ref, slow_ref, shift_ref, wr_ref, wi_ref,
    saved_ref, merged_ref, drive_ref, prev_ref, state_ref, reset_ref, norm_ref, inp_ref,
):
    rows, width = conv_ref.shape
    heads, hd = wr_ref.shape[0], wr_ref.shape[1]
    for h in range(heads):
        cols = slice(h * hd, (h + 1) * hd)
        conv = conv_ref[:, cols]
        reset = jax.nn.sigmoid(dot(conv, wr_ref[h]))
        inp = jax.nn.sigmoid(dot(conv, wi_ref[h]))
        log_decay = -8.0 * reset * slow_ref[:, cols] + shift_ref[...]
        decay = jnp.exp(log_decay)
        twice = 2.0 * log_decay
        small = jnp.maximum(twice, -0.5)
        series = 1.0 + small * (1.0 / 10.0)
        for n in (9, 8, 7, 6, 5, 4, 3, 2):
            series = 1.0 + small * (1.0 / n) * series
        less = jnp.where(twice > -0.5, small * series, jnp.exp(twice) - 1.0)
        norm = jnp.sqrt(-less)
        saved_ref[0, :, cols] = decay
        reset_ref[:, cols] = reset
        norm_ref[:, cols] = norm
        inp_ref[:, cols] = inp
        drive_ref[:, cols] = norm * inp * conv.astype(F32)

    def step(group, state):
        for i in range(8):
            t = pl.ds(group * 8 + i, 1)
            prev_ref[t, :] = state
            state = saved_ref[0, t, :] * state + drive_ref[t, :]
            state_ref[t, :] = state
        return state

    lax.fori_loop(0, rows // 8, step, first_ref[...])

    def back(group, prod):
        for i in range(8):
            t = rows - 1 - (group * 8 + i)
            saved_ref[1, pl.ds(t, 1), :] = prod
            prod = prod * saved_ref[0, pl.ds(t, 1), :]
        return prod

    lax.fori_loop(0, rows // 8, back, jnp.ones((1, width), F32))

    for h in range(heads):
        cols = slice(h * hd, (h + 1) * hd)
        conv = conv_ref[:, cols].astype(F32)
        decay, reset, norm, inp = saved_ref[0, :, cols], reset_ref[:, cols], norm_ref[:, cols], inp_ref[:, cols]
        by_log = decay * prev_ref[:, cols] - inp * conv * decay * decay / norm
        saved_ref[2, :, cols] = by_log * (-8.0 * slow_ref[:, cols]) * reset * (1.0 - reset)
        saved_ref[3, :, cols] = norm * conv * inp * (1.0 - inp)
        saved_ref[4, :, cols] = norm * inp
        state = state_ref[:, cols]
        value = gate_ref[:, cols].astype(F32)
        k = 0.7978845608028654
        square = value * value
        bent = jnp.tanh(k * (value + 0.044715 * value * square))
        act = 0.5 * value * (1.0 + bent)
        slope = 0.5 * (1.0 + bent) + 0.5 * value * (1.0 - bent * bent) * k * (1.0 + 3.0 * 0.044715 * square)
        saved_ref[5, :, cols] = state * slope
        saved_ref[6, :, cols] = act
        merged_ref[:, cols] = (act * state).astype(BF16)


def forward(conv, gate_in, first, slow, shift, w_reset, w_input):
    rows, width = conv.shape
    return pl.pallas_call(
        forward_kernel,
        out_shape=(
            jax.ShapeDtypeStruct((7, rows, width), F32),
            jax.ShapeDtypeStruct((rows, width), BF16),
        ),
        in_specs=[VM] * 7,
        out_specs=(VM, VM),
        scratch_shapes=[pltpu.VMEM((rows, width), F32)] * 6,
        name="forward_recurrence",
    )(conv, gate_in, first, slow, shift, w_reset, w_input)


def slot_tests(codes, experts):
    tokens = codes.shape[1]
    row = lax.broadcasted_iota(jnp.int32, (experts * 8, tokens), 0)
    base = (row // 8) * 16
    main = base + row % 8
    tail = base + 8 + row % 4
    return [[codes[k : k + 1, :] == want for k in (0, 1)] for want in (main, tail)], row % 8 < 4


def pack_kernel(ids_ref, wts_ref, d_out_ref, mixed_ref, send_ref, code_ref):
    experts = send_ref.shape[0]
    tokens, width = d_out_ref.shape
    half = width // 2
    each = lax.broadcasted_iota(jnp.int32, (experts, tokens), 0)
    named = [ids_ref[k : k + 1, :] == each for k in (0, 1)]
    both = jnp.where(named[0] | named[1], 1.0, 0.0).astype(BF16)
    earlier = (
        lax.broadcasted_iota(jnp.int32, (tokens, tokens), 0)
        < lax.broadcasted_iota(jnp.int32, (tokens, tokens), 1)
    )
    count = dot(both, jnp.where(earlier, 1.0, 0.0).astype(BF16))
    codes = []
    for k in (0, 1):
        rank = jnp.sum(jnp.where(named[k], count, 0.0), axis=0, keepdims=True)
        codes.append(ids_ref[k : k + 1, :] * 16 + rank.astype(jnp.int32))
        code_ref[k : k + 1, :] = codes[k]
    codes = jnp.concatenate(codes, axis=0)
    (main, tail), low = slot_tests(codes, experts)

    def weight(tests):
        return jnp.sum(
            jnp.where(tests[0], wts_ref[0:1, :], 0.0) + jnp.where(tests[1], wts_ref[1:2, :], 0.0),
            axis=1,
            keepdims=True,
        )

    main_pick = jnp.where(main[0] | main[1], 1.0, 0.0).astype(BF16)
    in_tail = tail[0] | tail[1]
    low_pick = jnp.where(in_tail & low, 1.0, 0.0).astype(BF16)
    high_pick = jnp.where(in_tail & ~low, 1.0, 0.0).astype(BF16)

    for at, (ref, w_main, w_tail) in enumerate(
        ((d_out_ref, weight(main), weight(tail)), (mixed_ref, None, None))
    ):
        first = dot(main_pick, ref[...])
        second = dot(low_pick, ref[:, :half]) + dot(high_pick, ref[:, half:])
        if w_main is not None:
            first, second = first * w_main, second * w_tail
        rows = slice(at * 8, at * 8 + 8)
        send_ref[:, rows, :width] = first.reshape(experts, 8, width).astype(BF16)
        send_ref[:, rows, width:] = second.reshape(experts, 8, half).astype(BF16)


def pack(ids, wts, d_out, mixed, experts):
    tokens, width = d_out.shape
    return pl.pallas_call(
        pack_kernel,
        out_shape=(
            jax.ShapeDtypeStruct((experts, 16, width + width // 2), BF16),
            jax.ShapeDtypeStruct((2, tokens), jnp.int32),
        ),
        in_specs=[VM] * 4,
        out_specs=(VM, VM),
        name="pack_slots",
    )(ids, wts, d_out, mixed)


def place():
    sp, tp = lax.axis_index("sp"), lax.axis_index("tp")
    return sp, tp, sp // 8, (sp // 2) % 4, sp % 2


def offset_device(z, x, c, dz, j):
    return ((z + dz) % 8) * 8 + ((x + j // 2) % 4) * 2 + (c + j % 2) % 2


def greet(sp, tp, n_sp, n_tp):
    barrier = pltpu.get_barrier_semaphore()

    def to_sp(k, _):
        pl.semaphore_signal(barrier, inc=1, device_id=((sp + k) % n_sp, tp), device_id_type=MESH)
        return 0

    lax.fori_loop(1, n_sp, to_sp, 0)
    for k in range(1, n_tp):
        pl.semaphore_signal(barrier, inc=1, device_id=(sp, (tp + k) % n_tp), device_id_type=MESH)
    pl.semaphore_wait(barrier, n_sp - 1 + n_tp - 1)


def remote(src, dst, send_sem, recv_sem, sp, tp):
    return pltpu.make_async_remote_copy(
        src_ref=src, dst_ref=dst, send_sem=send_sem, recv_sem=recv_sem,
        device_id=(sp, tp), device_id_type=MESH,
    )


def wait_bytes(ref, sem):
    pltpu.make_async_copy(ref, ref, sem).wait()


def dispatch_kernel(n_tp, send_ref, got_ref, own_sem, send_sem, recv_sem, y_send, y_recv, f_send, f_recv):
    sp, tp, z, x, c = place()
    n_sp = send_ref.shape[0]
    right, left, far = (tp + 1) % n_tp, (tp + n_tp - 1) % n_tp, (tp + 2) % n_tp
    greet(sp, tp, n_sp, n_tp)
    own = pltpu.make_async_copy(send_ref.at[sp], got_ref.at[tp, sp], own_sem)
    own.start()
    for i, dz in enumerate(Z_ORDER):

        def send(j, _):
            to = offset_device(z, x, c, dz, j)
            remote(send_ref.at[to], got_ref.at[tp, sp], send_sem, recv_sem.at[i], to, tp).start()
            return 0

        lax.fori_loop(1 if dz == 0 else 0, 8, send, 0)

    def group(i):
        return ((z + 8 - Z_ORDER[i]) % 8) * 8

    def forward_on(i):
        at = group(i)
        wait_bytes(got_ref.at[left, pl.ds(at, 8)], y_recv.at[0, i])
        part = got_ref.at[left, pl.ds(at, 4)]
        remote(part, part, f_send.at[0], f_recv.at[0, i], sp, right).start()
        wait_bytes(got_ref.at[right, pl.ds(at, 8)], y_recv.at[1, i])
        part = got_ref.at[right, pl.ds(at + 4, 4)]
        remote(part, part, f_send.at[1], f_recv.at[1, i], sp, left).start()

    for i in range(8):
        at = group(i)
        if i == 0:
            own.wait()
            wait_bytes(got_ref.at[tp, pl.ds(at, 7)], recv_sem.at[i])
        else:
            wait_bytes(got_ref.at[tp, pl.ds(at, 8)], recv_sem.at[i])
        part = got_ref.at[tp, pl.ds(at, 8)]
        remote(part, part, y_send.at[0], y_recv.at[0, i], sp, right).start()
        remote(part, part, y_send.at[1], y_recv.at[1, i], sp, left).start()
        if i > 0:
            forward_on(i - 1)
    forward_on(7)
    for i in range(8):
        at = group(i)
        wait_bytes(got_ref.at[far, pl.ds(at, 4)], f_recv.at[0, i])
        wait_bytes(got_ref.at[far, pl.ds(at + 4, 4)], f_recv.at[1, i])
    wait_bytes(send_ref.at[pl.ds(0, n_sp - 1)], send_sem)
    for side in (0, 1):
        wait_bytes(got_ref.at[tp], y_send.at[side])
        wait_bytes(got_ref.at[tp, pl.ds(0, n_sp // 2)], f_send.at[side])


def dispatch(send, n_tp):
    dma = pltpu.SemaphoreType.DMA
    return pl.pallas_call(
        functools.partial(dispatch_kernel, n_tp),
        out_shape=jax.ShapeDtypeStruct((n_tp, *send.shape), BF16),
        in_specs=[VM],
        out_specs=ANY,
        scratch_shapes=[dma, dma, dma((8,)), dma((2,)), dma((2, 8)), dma((2,)), dma((2, 8))],
        compiler_params=pltpu.CompilerParams(collective_id=0, has_side_effects=True),
        name="dispatch",
    )(send)


def expert_kernel(
    got_ref, wg_ref, wu_ref, wd_ref, gg_ref, gu_ref, gd_ref, part_ref,
    rows_ref, cot_ref, grad_ref, hidden_ref,
):
    n_tp, n_src = got_ref.shape[0], got_ref.shape[1]
    width = got_ref.shape[3] * 2 // 3
    half = width // 2
    fe = wg_ref.shape[1]
    main_rows = n_src * 8

    for q in range(n_tp):
        cols = slice(q * width, (q + 1) * width)

        def unpack(g, _):
            src = pl.ds(g * 16, 16)
            for at, ref in ((0, cot_ref), (8, rows_ref)):
                ref[pl.ds(g * 128, 128), cols] = (
                    got_ref[q, src, at : at + 8, :width].astype(F32).reshape(128, width).astype(BF16)
                )
                tails = got_ref[q, src, at : at + 8, width:].astype(F32)
                turned = swap4(tails)
                tails, turned = tails.reshape(8, 2, 8, half), turned.reshape(8, 2, 8, half)
                low = low_half((8, 8, half))
                left = jnp.where(low, tails[:, 0], turned[:, 1])
                right = jnp.where(low, turned[:, 0], tails[:, 1])
                both = jnp.concatenate([left, right], axis=2).reshape(64, width).astype(BF16)
                ref[pl.ds(main_rows + g * 64, 64), cols] = both
            return 0

        lax.fori_loop(0, n_src // 16, unpack, 0)

    def terms(r, _):
        rows = pl.ds(r * 256, 256)
        value = rows_ref[rows, :]
        up_pre = dot(value, wg_ref[...])
        linear = dot(value, wu_ref[...])
        d_hidden = dot(cot_ref[rows, :], wd_ref[...], ((1,), (1,)))
        gate = jax.nn.sigmoid(up_pre)
        silu = up_pre * gate
        hidden_ref[rows, :] = (silu * linear).astype(BF16)
        grad_ref[rows, fe:] = (d_hidden * silu).astype(BF16)
        grad_ref[rows, :fe] = (d_hidden * linear * gate * (1.0 + up_pre * (1.0 - gate))).astype(BF16)
        return 0

    lax.fori_loop(0, rows_ref.shape[0] // 256, terms, 0)

    for q in range(n_tp):
        cols = slice(q * width, (q + 1) * width)

        def part_of(rows):
            return dot(grad_ref[rows, :fe], wg_ref[cols, :], ((1,), (1,))) + dot(
                grad_ref[rows, fe:], wu_ref[cols, :], ((1,), (1,))
            )

        def first(r, _):
            part = part_of(pl.ds(r * 256, 256)).reshape(32, 8, width)
            part_ref[q, pl.ds(r * 32, 32), :, :width] = part.astype(BF16)
            return 0

        lax.fori_loop(0, main_rows // 256, first, 0)

        def second(r, _):
            part = part_of(pl.ds(main_rows + r * 128, 128)).reshape(16, 8, width)
            left, right = part[:, :, :half], part[:, :, half:]
            low = low_half((16, 8, half))
            one = jnp.where(low, left, swap4(right))
            two = jnp.where(low, swap4(left), right)
            both = jnp.stack([one, two], axis=1).reshape(32, 8, half)
            part_ref[q, pl.ds(r * 32, 32), :, width:] = both.astype(BF16)
            return 0

        lax.fori_loop(0, n_src // 32, second, 0)

    def weight_grads(k, _):
        cols = pl.ds(pl.multiple_of(k * 512, 512), 512)
        both = dot(rows_ref[:, cols], grad_ref[...], ((0,), (0,)))
        gg_ref[cols, :] = both[:, :fe]
        gu_ref[cols, :] = both[:, fe:]
        gd_ref[:, cols] = dot(hidden_ref[...], cot_ref[:, cols], ((0,), (0,)))
        return 0

    lax.fori_loop(0, rows_ref.shape[1] // 512, weight_grads, 0)


def experts_back(got, w_gate, w_up, w_down):
    n_tp, n_src, _, packed = got.shape
    model, fe = w_gate.shape
    rows = n_src * 12
    return pl.pallas_call(
        expert_kernel,
        out_shape=(
            jax.ShapeDtypeStruct((model, fe), F32),
            jax.ShapeDtypeStruct((model, fe), F32),
            jax.ShapeDtypeStruct((fe, model), F32),
            jax.ShapeDtypeStruct((n_tp, n_src, 8, packed), BF16),
        ),
        in_specs=[VM] * 4,
        out_specs=(VM,) * 4,
        scratch_shapes=[
            pltpu.VMEM((rows, model), BF16),
            pltpu.VMEM((rows, model), BF16),
            pltpu.VMEM((rows, 2 * fe), BF16),
            pltpu.VMEM((rows, fe), BF16),
        ],
        compiler_params=pltpu.CompilerParams(vmem_limit_bytes=56 * 2**20),
        name="experts",
    )(got, w_gate, w_up, w_down)


def tail_kernel(
    part_ref, code_ref, d_out_ref, saved_ref, merged_ref, w_out_ref, wr_ref, wi_ref,
    proj_ref, rec_ref, gate_ref,
    term_ref, back_ref, ret_ref, mix_ref, acc_ref, local_ref, keep_ref, pair_ref, pair_got,
    x_ref, x_got, z_ref, z_got, own_ref, lead_ref, lead_got,
    term_send, term_recv, ret_send, ret_recv, mix_send, mix_recv, pair_send, pair_recv,
    x_send, x_recv, z_send, z_recv, lead_send, lead_recv,
):
    sp, tp, z, x, c = place()
    n_tp, n_sp = part_ref.shape[0], part_ref.shape[1]
    tokens, width = d_out_ref.shape
    half = width // 2
    greet(sp, tp, n_sp, n_tp)

    for i, dz in enumerate(Z_ORDER):
        at = ((z + dz) % 8) * 8
        for k in (1, 3, 2):
            to = (tp + k) % n_tp
            remote(
                part_ref.at[to, pl.ds(at, 8)], term_ref.at[k - 1, i],
                term_send.at[k - 1], term_recv.at[k - 1, i], sp, to,
            ).start()
    for i, dz in enumerate(Z_ORDER):
        at = ((z + dz) % 8) * 8
        total = part_ref[tp, pl.ds(at, 8)].astype(F32)
        for k in range(1, n_tp):
            wait_bytes(term_ref.at[k - 1, i], term_recv.at[k - 1, i])
            total = total + term_ref[k - 1, i].astype(F32)
        back_ref[pl.ds(at, 8)] = total.astype(BF16)

        def send(j, _):
            to = offset_device(z, x, c, dz, j)
            remote(back_ref.at[to], ret_ref.at[sp], ret_send, ret_recv, to, tp).start()
            return 0

        lax.fori_loop(1 if dz == 0 else 0, 8, send, 0)
    ret_ref[sp] = back_ref[sp]
    wait_bytes(ret_ref.at[pl.ds(0, n_sp - 1)], ret_recv)

    (main, tail), low = slot_tests(code_ref[...], n_sp)
    main_pick = jnp.where(main[0] | main[1], 1.0, 0.0).astype(BF16)
    in_tail = tail[0] | tail[1]
    low_pick = jnp.where(in_tail & low, 1.0, 0.0).astype(BF16)
    high_pick = jnp.where(in_tail & ~low, 1.0, 0.0).astype(BF16)
    first = ret_ref[:, :, :width].astype(F32).reshape(n_sp * 8, width).astype(BF16)
    second = ret_ref[:, :, width:].astype(F32).reshape(n_sp * 8, half).astype(BF16)
    rows = ((0,), (0,))
    summed = dot(main_pick, first, rows) + jnp.concatenate(
        [dot(low_pick, second, rows), dot(high_pick, second, rows)], axis=1
    )
    mix_ref[tp] = (d_out_ref[...].astype(F32) + summed).astype(BF16)
    for k in (1, 3, 2):
        to = (tp + k) % n_tp
        remote(mix_ref.at[tp], mix_ref.at[tp], mix_send.at[k - 1], mix_recv.at[k - 1], sp, to).start()

    def number(k, h):
        return 2 * ((tp + n_tp - k) % n_tp) + h

    slot_of = (0, 1, 3, 2)
    for n, k in enumerate(slot_of):
        q = (tp + n_tp - k) % n_tp
        if k:
            wait_bytes(mix_ref.at[q], mix_recv.at[k - 1])
        mixed = mix_ref[q]
        block = dot(mixed, w_out_ref[:, pl.ds(pl.multiple_of(q * width, width), width)], ((1,), (1,)))
        if n == 0:
            acc_ref[...] = block
        else:
            acc_ref[...] += block
        for h in (0, 1):
            slot = 2 * n + h
            grad = dot(mixed[:, h * half : (h + 1) * half], merged_ref[...], rows)
            grad = grad.reshape(4, 2, half // 8, width)
            keep_ref[slot] = jnp.where(c == 0, grad[:, 0], grad[:, 1])
            pair_ref[slot] = jnp.where(c == 0, grad[:, 1], grad[:, 0]).astype(BF16)
            remote(
                pair_ref.at[slot], pair_got.at[slot], pair_send, pair_recv.at[slot], sp + 1 - 2 * c, tp
            ).start()

    d_merged = acc_ref[...]
    gate_ref[...] = (d_merged * saved_ref[5]).astype(BF16)
    acc_ref[...] = d_merged * saved_ref[6]

    def back(group, carry):
        for i in range(8):
            t = pl.ds(tokens - 1 - (group * 8 + i), 1)
            grad = acc_ref[t, :] + carry
            local_ref[t, :] = grad
            carry = grad * saved_ref[0, t, :]
        return carry

    lead = lax.fori_loop(0, tokens // 8, back, jnp.zeros((1, width), F32))
    lead_ref[0, 0:1, :] = saved_ref[1, 0:1, :] * saved_ref[0, 0:1, :]
    lead_ref[0, 1:2, :] = lead
    lead_got[sp] = lead_ref[0]

    def tell(k, _):
        remote(lead_ref.at[0], lead_got.at[sp], lead_send, lead_recv, (sp + k) % n_sp, tp).start()
        return 0

    lax.fori_loop(1, n_sp, tell, 0)

    for slot in range(8):
        wait_bytes(pair_got.at[slot], pair_recv.at[slot])
        total = keep_ref[slot] + pair_got[slot].astype(F32)
        keep_ref[slot] = total
        x_ref[slot] = total.astype(BF16)
        for dx in (1, 3, 2):
            to = (x + dx) % 4
            remote(
                x_ref.at[slot, to], x_got.at[slot, dx - 1], x_send, x_recv.at[slot],
                z * 8 + to * 2 + c, tp,
            ).start()

    for slot in range(8):
        wait_bytes(x_got.at[slot], x_recv.at[slot])
        total = keep_ref[slot, x] + x_got[slot, 0].astype(F32) + x_got[slot, 1].astype(F32) + x_got[slot, 2].astype(F32)
        z_ref[slot] = total.astype(BF16)
        to = number(slot_of[slot // 2], slot % 2)

        @pl.when(to == z)
        def _():
            own_ref[...] = total

        @pl.when(to != z)
        def _():
            remote(z_ref.at[slot], z_got.at[z], z_send, z_recv, to * 8 + x * 2 + c, tp).start()

    wait_bytes(lead_got.at[pl.ds(0, n_sp - 1)], lead_recv)

    def later(k, carry):
        i = n_sp - 1 - k
        pair = lead_got[i]
        return jnp.where(i > sp, pair[1:2, :] + pair[0:1, :] * carry, carry)

    incoming = lax.fori_loop(0, n_sp, later, jnp.zeros((1, width), F32))
    heads, hd = wr_ref.shape[0], wr_ref.shape[1]
    for h in range(heads):
        cols = slice(h * hd, (h + 1) * hd)
        grad = local_ref[:, cols] + saved_ref[1, :, cols] * incoming[:, cols]
        by_reset = (grad * saved_ref[2, :, cols]).astype(BF16)
        by_input = (grad * saved_ref[3, :, cols]).astype(BF16)
        rec_ref[:, cols] = (
            grad * saved_ref[4, :, cols]
            + dot(by_reset, wr_ref[h], ((1,), (1,)))
            + dot(by_input, wi_ref[h], ((1,), (1,)))
        ).astype(BF16)

    wait_bytes(z_got.at[pl.ds(0, 7)], z_recv)
    total = own_ref[...]
    for d in range(1, 8):
        total = total + z_got[(z + d) % 8].astype(F32)
    proj_ref[...] = total

    for k in range(n_tp - 1):
        wait_bytes(part_ref.at[tp], term_send.at[k])
        wait_bytes(mix_ref.at[tp], mix_send.at[k])
    wait_bytes(back_ref.at[pl.ds(0, n_sp - 1)], ret_send)
    wait_bytes(pair_ref, pair_send)
    wait_bytes(x_ref.at[:, pl.ds(0, 3)], x_send)
    wait_bytes(z_ref.at[pl.ds(0, 7)], z_send)
    wait_bytes(lead_got.at[pl.ds(0, n_sp - 1)], lead_send)


def tail(part, codes, d_out, saved, merged, w_out, w_reset, w_input):
    n_tp, n_sp, _, packed = part.shape
    tokens, width = d_out.shape
    own_rows = n_tp * width // n_sp
    dma = pltpu.SemaphoreType.DMA
    block = (own_rows, width)
    return pl.pallas_call(
        tail_kernel,
        out_shape=(
            jax.ShapeDtypeStruct(block, F32),
            jax.ShapeDtypeStruct((tokens, width), BF16),
            jax.ShapeDtypeStruct((tokens, width), BF16),
        ),
        in_specs=[VM] * 8,
        out_specs=(VM,) * 3,
        scratch_shapes=[
            pltpu.VMEM((3, 8, 8, 8, packed), BF16),
            pltpu.VMEM((n_sp, 8, packed), BF16),
            pltpu.VMEM((n_sp, 8, packed), BF16),
            pltpu.VMEM((n_tp, tokens, width), BF16),
            pltpu.VMEM((tokens, width), F32),
            pltpu.VMEM((tokens, width), F32),
            pltpu.VMEM((8, 4, *block), F32),
            pltpu.VMEM((8, 4, *block), BF16),
            pltpu.VMEM((8, 4, *block), BF16),
            pltpu.VMEM((8, 4, *block), BF16),
            pltpu.VMEM((8, 3, *block), BF16),
            pltpu.VMEM((8, *block), BF16),
            pltpu.VMEM((8, *block), BF16),
            pltpu.VMEM(block, F32),
            pltpu.VMEM((1, 2, width), F32),
            pltpu.VMEM((n_sp, 2, width), F32),
            dma((3,)), dma((3, 8)), dma, dma, dma((3,)), dma((3,)), dma, dma((8,)),
            dma, dma((8,)), dma, dma, dma, dma,
        ],
        compiler_params=pltpu.CompilerParams(
            collective_id=1, has_side_effects=True, vmem_limit_bytes=56 * 2**20
        ),
        name="return_and_tail",
    )(part, codes, d_out, saved, merged, w_out, w_reset, w_input)


def body(
    n_sp, n_tp, conv_out, gate_in, block_states, decay_param, decay_shift, w_reset, w_input, w_out,
    mixed, d_out, expert_ids, route_weights, w_gate, w_up, w_down,
):
    slow = jax.nn.softplus(-decay_param)[None, :]
    send, codes = pack(expert_ids.T, route_weights.T, d_out, mixed, n_sp)
    got = dispatch(send, n_tp)
    saved, merged = forward(conv_out, gate_in, block_states, slow, decay_shift[:, None], w_reset, w_input)
    grad_gate_e, grad_up_e, grad_down_e, part = experts_back(got, w_gate[0], w_up[0], w_down[0])
    proj, rec, grad_gate = tail(part, codes, d_out, saved, merged, w_out, w_reset, w_input)
    return grad_gate_e[None], grad_up_e[None], grad_down_e[None], proj, rec, grad_gate


def solution(mesh):
    in_specs = (
        P("sp", "tp"), P("sp", "tp"), P("sp", "tp"), P("tp"), P("sp"),
        P("tp", None, None), P("tp", None, None), P("tp", None),
        P("sp", "tp"), P("sp", "tp"), P("sp", None), P("sp", None),
        P("sp", None, "tp"), P("sp", None, "tp"), P("sp", "tp", None),
    )
    out_specs = (
        P("sp", None, "tp"), P("sp", None, "tp"), P("sp", "tp", None),
        P("sp", "tp"), P("sp", "tp"), P("sp", "tp"),
    )
    run = functools.partial(body, mesh.shape["sp"], mesh.shape["tp"])
    return jax.shard_map(run, mesh=mesh, in_specs=in_specs, out_specs=out_specs, check_vma=False)
```

time: 508 us -> 199 us (0.39); the launches traced: 501 us -> 199 us
  Pallas kernels: 0 us -> 192 us
  local copies, waits for them, and re-layouts: 173 us -> 5.49 us
  waiting for transfers between devices: 135 us -> 0 us
  other arithmetic: 59.6 us -> 0.61 us
  blocking collectives: 51.8 us -> 0 us
  starting transfers between devices: 33.5 us -> 0 us
  matrix products: 32.4 us -> 0 us
  between operations: 15.3 us -> 0.67 us
    pallas_call x0 -> x5, Pallas kernels: none -> 192 us  [the longest x1 88.8 us: tail(): pl.pallas_call(tail_kernel, out_shape=(jax.ShapeDtypeStruct(block, F32),...]
    slice x129 -> x0, local copies, waits for them, and re-layouts: 97.4 us -> none  [the longest x53 68.3 us: body(): lax.associative_scan(decay_combine, (next_decay[::-1], d_states[::-1]), a...]
    all_gather x1 -> x0, waiting for transfers between devices: 68.1 us -> none  [side_by_side(): filled, at, done = (lax.all_gather(both, axis, axis=dim, tiled=True), 0, [])]
    all_to_all x1 -> x0, blocking collectives: 51.8 us -> none  [in_one_piece(): lax.all_to_all(both, axis, split_axis=split_dim, concat_axis=concat_dim,...]
    reduce_scatter x3 -> x0, waiting for transfers between devices: 33.7 us -> none  [own_rows(): so_far = lax.psum_scatter(so_far, axis, scatter_dimension=0, tiled=True)]
    all_to_all x4 -> x0, starting transfers between devices: 33.2 us -> none  [the longest x2 16.5 us: copy_for_each(): lax.all_to_all(jnp.broadcast_to(value[None], (devices, *value.shape)), ax...]
    all_to_all x4 -> x0, waiting for transfers between devices: 32.9 us -> none  [the longest x1 32.9 us: sent_and_summed(): lax.all_to_all(split_up(value, dim, devices), axis, 0, 0, tiled=True)]
    dot_general x14 -> x0, matrix products: 32.4 us -> none  [the longest x4 14.5 us: over_rows(): lax.dot_general(left_matrix, right_matrix, (((0,), (0,)), ((), ())), pref...]
  transfers between devices with their start and end apart: 8 -> 0, of which waited for: 4 -> 0; matrix products, arithmetic and copies ran while one was open for 23% -> 0% of each run, Pallas kernels for 0% -> 0%
where the time goes in v1:
time: 199 us
  Pallas kernels  192 us (96%)
  local copies, waits for them, and re-layouts  5.49 us (3%)
    pallas_call x1, Pallas kernels, tail(): pl.pallas_call(tail_kernel, out_shape=(jax.ShapeDtypeStruct(block, F32),...  88.8 us
    pallas_call x1, Pallas kernels, dispatch(): pl.pallas_call(functools.partial(dispatch_kernel, n_tp), out_shape=jax.Sh...  75.6 us
    pallas_call x1, Pallas kernels, experts_back(): pl.pallas_call(expert_kernel, out_shape=(jax.ShapeDtypeStruct((model, fe)...  18.8 us
    pallas_call x1, Pallas kernels, forward(): pl.pallas_call(forward_kernel, out_shape=(jax.ShapeDtypeStruct((7, rows,...  5.57 us
    unnamed x7, local copies, waits for them, and re-layouts  4.72 us

profile of v1, /device:TPU:16, one launch (start us, length us, event | category | flops | bytes accessed | tf_op | source)
XLA Modules:
  0.0 198.9 jit_solution(1989508912390930695)
XLA Ops:
  0.6 3.3 %pack_slots.1 = (bf16[64,16,768]{2,1,0:T(8,128)(2,1)}, s32[2,192]{1,0:T(2,128)}) custom-call(s32[2,192]{1,0:T(2,128)} %bitcast.14, f32[2,192]{1,0:T(2,128)} %bitcast.15, bf16[192,512]{1,0:T(8,128)(2,1)} %d_out_ref.3, bf16[192,512]{1,0:T(8,128)(2,1)} %mixed_ref.1), custom_call_target="tpu_custom_call" | custom-call | tf_op jit(solution)/shard_map/pack_slots/pallas_call | solution.py:165
  4.0 75.6 %dispatch.1.got_ref = bf16[4,64,16,768]{3,2,1,0:T(8,128)(2,1)} custom-call(bf16[64,16,768]{2,1,0:T(8,128)(2,1)} %get-tuple-element.17.send_ref), custom_call_target="tpu_custom_call" | custom-call | tf_op jit(solution)/shard_map/dispatch/pallas_call | solution.py:263
  79.6 0.0 copy-start.1
  79.6 0.0 copy-start
  79.6 18.8 %experts.1 = (f32[2048,256]{1,0:T(8,128)}, f32[2048,256]{1,0:T(8,128)}, f32[256,2048]{1,0:T(8,128)}, bf16[4,64,8,768]{3,2,1,0:T(8,128)(2,1)}) custom-call(bf16[4,64,16,768]{3,2,1,0:T(8,128)(2,1)} %dispatch.1.got_ref, bf16[2048,256]{1,0:T(8,128)(2,1)} %bitcast.10, bf16[2048,256]{1,0:T(8,128)(2,1)} %bitcast.11, bf16[256,2048]{1,0:T(8,128)(2,1)} %bitcast.12), custom_call_target="tpu_custom_call" | custom-call | tf_op jit(solution)/shard_map/experts/pallas_call | solution.py:362
  98.4 0.0 copy-done.1
  98.4 0.8 copy.21.shift_ref
  99.2 0.0 copy-done
  99.2 0.6 compare_select_fusion
  99.8 5.6 %forward_recurrence.1 = (f32[7,192,512]{2,1,0:T(8,128)}, bf16[192,512]{1,0:T(8,128)(2,1)}) custom-call(bf16[192,512]{1,0:T(8,128)(2,1)} %conv_ref.1, bf16[192,512]{1,0:T(8,128)(2,1)} %gate_ref.1, f32[1,512]{1,0:T(1,128)} %first_ref.1, f32[1,512]{1,0:T(1,128)} %bitcast.13, f32[192,1]{1,0:T(8,128)} %copy.21.shift_ref, bf16[4,128,128]{2,1,0:T(8,128)(2,1)} %wr_ref.3, ...), custom_call_target="tpu_custom_call" | custom-call | tf_op jit(solution)/shard_map/forward_recurrence/pallas_call | solution.py:97
  105.4 88.8 %return_and_tail.1 = (f32[32,512]{1,0:T(8,128)}, bf16[192,512]{1,0:T(8,128)(2,1)}, bf16[192,512]{1,0:T(8,128)(2,1)}) custom-call(bf16[4,64,8,768]{3,2,1,0:T(8,128)(2,1)} %get-tuple-element.21.part_ref, s32[2,192]{1,0:T(2,128)} %get-tuple-element.22.code_ref, bf16[192,512]{1,0:T(8,128)(2,1)} %d_out_ref.3, f32[7,192,512]{2,1,0:T(8,128)} %get-tuple-element.23.saved_ref, ...), custom_call_target="tpu_custom_call" | custom-call | tf_op jit(solution)/shard_map/return_and_tail/pallas_call | solution.py:553
  194.2 1.5 copy.25
  195.7 1.6 copy.26
  197.3 1.6 copy.27
Async XLA Ops:
  79.6 18.8 %copy-start.1 = (f32[192]{0:T(256)S(1)}, f32[192]{0:T(256)}, u32[]{:S(2)}) copy-start(f32[192]{0:T(256)} %param.19) | copy-start | bytes 2308
  79.6 19.6 %copy-start = (f32[512]{0:T(512)S(1)}, f32[512]{0:T(512)}, u32[]{:S(2)}) copy-start(f32[512]{0:T(512)} %param.18) | copy-start | bytes 6148

commit v2 on v1

v2 whole, which is shorter than its diff:
```python
import functools

import jax
import jax.numpy as jnp
from jax import lax
from jax.experimental import pallas as pl
from jax.experimental.pallas import tpu as pltpu
from jax.sharding import PartitionSpec as P

F32 = jnp.float32
BF16 = jnp.bfloat16
MESH = pl.DeviceIdType.MESH
VM = pl.BlockSpec(memory_space=pltpu.VMEM)
ANY = pl.BlockSpec(memory_space=pl.ANY)


def dot(a, b, dims=((1,), (0,))):
    return lax.dot_general(a, b, (dims, ((), ())), preferred_element_type=F32)


def swap4(value):
    return pltpu.roll(value, 4, axis=1)


def low_half(shape):
    return lax.broadcasted_iota(jnp.int32, shape, 1) < 4


def gates(conv_ref, slow_ref, shift_ref, wr_ref, wi_ref, saved_ref, drive_ref, reset_ref, norm_ref, inp_ref):
    hd = wr_ref.shape[1]
    rows = conv_ref.shape[0]
    shift = jnp.transpose(jnp.broadcast_to(shift_ref[...], (8, rows)))[:, 0:1]
    for h in range(wr_ref.shape[0]):
        cols = slice(h * hd, (h + 1) * hd)
        conv = conv_ref[:, cols]
        reset = jax.nn.sigmoid(dot(conv, wr_ref[h]))
        inp = jax.nn.sigmoid(dot(conv, wi_ref[h]))
        log_decay = -8.0 * reset * slow_ref[:, cols] + shift
        decay = jnp.exp(log_decay)
        twice = 2.0 * log_decay
        small = jnp.maximum(twice, -0.5)
        series = 1.0 + small * (1.0 / 10.0)
        for n in (9, 8, 7, 6, 5, 4, 3, 2):
            series = 1.0 + small * (1.0 / n) * series
        less = jnp.where(twice > -0.5, small * series, jnp.exp(twice) - 1.0)
        norm = jnp.sqrt(-less)
        saved_ref[0, :, cols] = decay
        reset_ref[:, cols] = reset
        norm_ref[:, cols] = norm
        inp_ref[:, cols] = inp
        drive_ref[:, cols] = norm * inp * conv.astype(F32)


def run_forward(first_ref, saved_ref, drive_ref, prev_ref, state_ref):
    rows, width = drive_ref.shape

    def step(group, state):
        for i in range(8):
            t = pl.ds(group * 8 + i, 1)
            prev_ref[t, :] = state
            state = saved_ref[0, t, :] * state + drive_ref[t, :]
            state_ref[t, :] = state
        return state

    lax.fori_loop(0, rows // 8, step, first_ref[...])

    def back(group, prod):
        for i in range(8):
            t = rows - 1 - (group * 8 + i)
            saved_ref[1, pl.ds(t, 1), :] = prod
            prod = prod * saved_ref[0, pl.ds(t, 1), :]
        return prod

    lax.fori_loop(0, rows // 8, back, jnp.ones((1, width), F32))


def factors(
    conv_ref, gate_ref, slow_ref, saved_ref, merged_ref, prev_ref, state_ref, reset_ref, norm_ref, inp_ref
):
    hd = 128
    for h in range(conv_ref.shape[1] // hd):
        cols = slice(h * hd, (h + 1) * hd)
        conv = conv_ref[:, cols].astype(F32)
        decay, reset, norm, inp = saved_ref[0, :, cols], reset_ref[:, cols], norm_ref[:, cols], inp_ref[:, cols]
        by_log = decay * prev_ref[:, cols] - inp * conv * decay * decay / norm
        saved_ref[2, :, cols] = by_log * (-8.0 * slow_ref[:, cols]) * reset * (1.0 - reset)
        saved_ref[3, :, cols] = norm * conv * inp * (1.0 - inp)
        saved_ref[4, :, cols] = norm * inp
        state = state_ref[:, cols]
        value = gate_ref[:, cols].astype(F32)
        k = 0.7978845608028654
        square = value * value
        bent = jnp.tanh(k * (value + 0.044715 * value * square))
        act = 0.5 * value * (1.0 + bent)
        slope = 0.5 * (1.0 + bent) + 0.5 * value * (1.0 - bent * bent) * k * (1.0 + 3.0 * 0.044715 * square)
        saved_ref[5, :, cols] = state * slope
        saved_ref[6, :, cols] = act
        merged_ref[:, cols] = (act * state).astype(BF16)


def slot_tests(codes, experts):
    tokens = codes.shape[1]
    row = lax.broadcasted_iota(jnp.int32, (experts * 8, tokens), 0)
    base = (row // 8) * 16
    main = base + row % 8
    tail = base + 8 + row % 4
    return [[codes[k : k + 1, :] == want for k in (0, 1)] for want in (main, tail)], row % 8 < 4


def pack(ids_ref, wts_ref, d_out_ref, mixed_ref, send_ref, code_ref):
    experts = send_ref.shape[0]
    tokens, width = d_out_ref.shape
    half = width // 2
    each = lax.broadcasted_iota(jnp.int32, (experts, tokens), 0)
    named = [ids_ref[k : k + 1, :] == each for k in (0, 1)]
    both = jnp.where(named[0] | named[1], 1.0, 0.0).astype(BF16)
    earlier = (
        lax.broadcasted_iota(jnp.int32, (tokens, tokens), 0)
        < lax.broadcasted_iota(jnp.int32, (tokens, tokens), 1)
    )
    count = dot(both, jnp.where(earlier, 1.0, 0.0).astype(BF16))
    codes = []
    for k in (0, 1):
        rank = jnp.sum(jnp.where(named[k], count, 0.0), axis=0, keepdims=True)
        codes.append(ids_ref[k : k + 1, :] * 16 + rank.astype(jnp.int32))
        code_ref[k : k + 1, :] = codes[k]
    codes = jnp.concatenate(codes, axis=0)
    (main, tail), low = slot_tests(codes, experts)

    def weight(tests):
        return jnp.sum(
            jnp.where(tests[0], wts_ref[0:1, :], 0.0) + jnp.where(tests[1], wts_ref[1:2, :], 0.0),
            axis=1,
            keepdims=True,
        )

    main_pick = jnp.where(main[0] | main[1], 1.0, 0.0).astype(BF16)
    in_tail = tail[0] | tail[1]
    low_pick = jnp.where(in_tail & low, 1.0, 0.0).astype(BF16)
    high_pick = jnp.where(in_tail & ~low, 1.0, 0.0).astype(BF16)

    for at, (ref, w_main, w_tail) in enumerate(
        ((d_out_ref, weight(main), weight(tail)), (mixed_ref, None, None))
    ):
        first = dot(main_pick, ref[...])
        second = dot(low_pick, ref[:, :half]) + dot(high_pick, ref[:, half:])
        if w_main is not None:
            first, second = first * w_main, second * w_tail
        rows = slice(at * 8, at * 8 + 8)
        send_ref[:, rows, :width] = first.reshape(experts, 8, width).astype(BF16)
        send_ref[:, rows, width:] = second.reshape(experts, 8, half).astype(BF16)


def place():
    sp, tp = lax.axis_index("sp"), lax.axis_index("tp")
    return sp, tp, sp // 8, (sp // 2) % 4, sp % 2


def z_offset(i):
    return ((i % 2) * ((i + 1) // 2) + (1 - i % 2) * (8 - i // 2)) % 8


def offset_device(z, x, c, dz, j):
    return ((z + dz) % 8) * 8 + ((x + j // 2) % 4) * 2 + (c + j % 2) % 2


def greet(sp, tp, n_sp, n_tp):
    barrier = pltpu.get_barrier_semaphore()

    def to_sp(k, _):
        pl.semaphore_signal(barrier, inc=1, device_id=((sp + k) % n_sp, tp), device_id_type=MESH)
        return 0

    lax.fori_loop(1, n_sp, to_sp, 0)
    for k in range(1, n_tp):
        pl.semaphore_signal(barrier, inc=1, device_id=(sp, (tp + k) % n_tp), device_id_type=MESH)


def all_here(n_sp, n_tp):
    pl.semaphore_wait(pltpu.get_barrier_semaphore(), n_sp - 1 + n_tp - 1)


def remote(src, dst, send_sem, recv_sem, sp, tp):
    return pltpu.make_async_remote_copy(
        src_ref=src, dst_ref=dst, send_sem=send_sem, recv_sem=recv_sem,
        device_id=(sp, tp), device_id_type=MESH,
    )


def wait_bytes(ref, sem):
    pltpu.make_async_copy(ref, ref, sem).wait()


def unpack(got_ref, q, at, row, rows_ref, cot_ref):
    packed = got_ref.shape[3]
    width, half = packed * 2 // 3, packed // 3
    cols = slice(q * width, (q + 1) * width)
    for first, ref in ((0, cot_ref), (8, rows_ref)):
        block = got_ref[q, pl.ds(at, 8), first : first + 8, :].astype(F32)
        ref[pl.ds(row, 64), cols] = block[:, :, :width].reshape(64, width).astype(BF16)
        tails = block[:, :, width:]
        turned = swap4(tails)
        tails, turned = tails.reshape(4, 2, 8, half), turned.reshape(4, 2, 8, half)
        low = low_half((4, 8, half))
        left = jnp.where(low, tails[:, 0], turned[:, 1])
        right = jnp.where(low, turned[:, 0], tails[:, 1])
        both = jnp.concatenate([left, right], axis=2).reshape(32, width)
        ref[pl.ds(row + 64, 32), cols] = both.astype(BF16)


def expert_terms(row, rows_ref, cot_ref, grad_ref, hidden_ref, wboth_ref, wd_ref):
    fe = wd_ref.shape[0]
    rows = pl.ds(row, 96)
    both = dot(rows_ref[rows, :], wboth_ref[...])
    up_pre, linear = both[:, :fe], both[:, fe:]
    d_hidden = dot(cot_ref[rows, :], wd_ref[...], ((1,), (1,)))
    gate = jax.nn.sigmoid(up_pre)
    silu = up_pre * gate
    hidden_ref[rows, :] = (silu * linear).astype(BF16)
    d_linear = (d_hidden * silu).astype(BF16)
    d_up = (d_hidden * linear * gate * (1.0 + up_pre * (1.0 - gate))).astype(BF16)
    grad_ref[rows, :fe] = d_up
    grad_ref[rows, fe:] = d_linear


def row_part(q, at, row, grad_ref, wboth_ref, part_ref):
    packed = part_ref.shape[3]
    width, half = packed * 2 // 3, packed // 3
    part = dot(grad_ref[pl.ds(row, 96), :], wboth_ref[q * width : (q + 1) * width, :], ((1,), (1,)))
    part_ref[q, pl.ds(at, 8), :, :width] = part[:64].reshape(8, 8, width).astype(BF16)
    tails = part[64:].reshape(4, 8, width)
    left, right = tails[:, :, :half], tails[:, :, half:]
    low = low_half((4, 8, half))
    one = jnp.where(low, left, swap4(right))
    two = jnp.where(low, swap4(left), right)
    part_ref[q, pl.ds(at, 8), :, width:] = jnp.stack([one, two], axis=1).reshape(8, 8, half).astype(BF16)


STAGES = (0, 2, 3, 4, 5)
GROUPS = 8


def step_kernel(
    conv_ref, gate_in_ref, first_ref, slow_ref, shift_ref, wr_ref, wi_ref, wo_hbm, mixed_ref, d_out_ref,
    ids_ref, wts_ref, wg_hbm, wu_hbm, wd_hbm,
    both_hbm, down_hbm, proj_ref, rec_ref, gate_ref,
    send_ref, code_ref, got_ref, rows_ref, cot_ref, grad_ref, hidden_ref, part_ref, far_ref, comb_ref,
    near_ref, back_ref, ret_ref, saved_ref, merged_ref, temp_ref, wboth_ref, wd_ref, wo_ref, both_ref,
    down_ref, mix_ref, acc_ref, local_ref, keep_ref, pair_ref, pair_got, x_ref, x_got, z_ref, z_got,
    own_ref, lead_ref, lead_got,
    load_sem, store_sem, send_sem, recv_sem, y_send, y_recv, f_send, f_recv, far_send, far_recv,
    near_send, near_recv, ret_send, ret_recv, mix_send, mix_recv, pair_send, pair_recv,
    x_send, x_recv, z_send, z_recv, lead_send, lead_recv,
):
    sp, tp, z, x, c = place()
    n_tp, n_sp = part_ref.shape[0], part_ref.shape[1]
    tokens, width = d_out_ref.shape
    half = width // 2
    fe = wd_ref.shape[0]
    right, left, far = (tp + 1) % n_tp, (tp + n_tp - 1) % n_tp, (tp + 2) % n_tp
    drive_ref, prev_ref, state_ref, reset_ref, norm_ref, inp_ref = [temp_ref.at[k] for k in range(6)]

    greet(sp, tp, n_sp, n_tp)
    loads = [
        pltpu.make_async_copy(src, dst, load_sem.at[k])
        for k, (src, dst) in enumerate((
            (wg_hbm, wboth_ref.at[:, pl.ds(0, fe)]), (wu_hbm, wboth_ref.at[:, pl.ds(fe, fe)]),
            (wd_hbm, wd_ref), (wo_hbm, wo_ref),
        ))
    ]
    for load in loads:
        load.start()
    pack(ids_ref, wts_ref, d_out_ref, mixed_ref, send_ref, code_ref)
    got_ref[tp, sp] = send_ref[sp]
    all_here(n_sp, n_tp)

    def send_group(i, _):
        def send(j, _):
            to = offset_device(z, x, c, z_offset(i), j)
            remote(send_ref.at[to], got_ref.at[tp, sp], send_sem, recv_sem.at[i], to, tp).start()
            return 0

        lax.fori_loop(jnp.where(i == 0, 1, 0), 8, send, 0)
        return 0

    lax.fori_loop(0, GROUPS, send_group, 0)

    def source_group(i):
        return (z + 8 - z_offset(i)) % 8

    def gather(i):
        at = source_group(i) * 8

        @pl.when(i == 0)
        def _():
            wait_bytes(got_ref.at[tp, pl.ds(at, 7)], recv_sem.at[i])

        @pl.when(i > 0)
        def _():
            wait_bytes(got_ref.at[tp, pl.ds(at, 8)], recv_sem.at[i])

        block = got_ref.at[tp, pl.ds(at, 8)]
        remote(block, block, y_send.at[0], y_recv.at[0, i], sp, right).start()
        remote(block, block, y_send.at[1], y_recv.at[1, i], sp, left).start()

    def relay(i):
        at = source_group(i) * 8
        wait_bytes(got_ref.at[left, pl.ds(at, 8)], y_recv.at[0, i])
        block = got_ref.at[left, pl.ds(at, 4)]
        remote(block, block, f_send.at[0], f_recv.at[0, i], sp, right).start()
        wait_bytes(got_ref.at[right, pl.ds(at, 8)], y_recv.at[1, i])
        block = got_ref.at[right, pl.ds(at + 4, 4)]
        remote(block, block, f_send.at[1], f_recv.at[1, i], sp, left).start()

    def compute(i):
        group = source_group(i)
        at, row = group * 8, pl.multiple_of(group * 96, 32)
        wait_bytes(got_ref.at[far, pl.ds(at, 4)], f_recv.at[0, i])
        wait_bytes(got_ref.at[far, pl.ds(at + 4, 4)], f_recv.at[1, i])
        for q in range(n_tp):
            unpack(got_ref, q, at, row, rows_ref, cot_ref)
        expert_terms(row, rows_ref, cot_ref, grad_ref, hidden_ref, wboth_ref, wd_ref)
        for q in range(n_tp):
            row_part(q, at, row, grad_ref, wboth_ref, part_ref)
        lower, upper = pl.ds(at, 4), pl.ds(at + 4, 4)
        remote(part_ref.at[far, lower], far_ref.at[0, i], far_send.at[0], far_recv.at[0, i], sp, left).start()
        remote(part_ref.at[far, upper], far_ref.at[1, i], far_send.at[1], far_recv.at[1, i], sp, right).start()
        remote(
            part_ref.at[left, upper], near_ref.at[0, i, pl.ds(4, 4)], near_send.at[0], near_recv.at[0, i], sp, left
        ).start()
        remote(
            part_ref.at[right, lower], near_ref.at[1, i, pl.ds(0, 4)], near_send.at[1], near_recv.at[1, i], sp, right
        ).start()

    def add_far(i):
        at = source_group(i) * 8
        for side, (to, first) in enumerate(((left, 0), (right, 4))):
            wait_bytes(far_ref.at[side, i], far_recv.at[side, i])
            own = part_ref[to, pl.ds(at + first, 4)].astype(F32)
            comb_ref[side, i] = (own + far_ref[side, i].astype(F32)).astype(BF16)
            remote(
                comb_ref.at[side, i], near_ref.at[side, i, pl.ds(first, 4)],
                near_send.at[side], near_recv.at[side, i], sp, to,
            ).start()

    def give_back(i):
        group = source_group(i)
        at = group * 8
        wait_bytes(near_ref.at[0, i], near_recv.at[0, i])
        wait_bytes(near_ref.at[1, i], near_recv.at[1, i])
        total = part_ref[tp, pl.ds(at, 8)].astype(F32) + near_ref[0, i].astype(F32) + near_ref[1, i].astype(F32)
        back_ref[pl.ds(at, 8)] = total.astype(BF16)

        def send(j, _):
            to = group * 8 + ((x + j // 2) % 4) * 2 + (c + j % 2) % 2
            remote(back_ref.at[to], ret_ref.at[sp], ret_send, ret_recv, to, tp).start()
            return 0

        lax.fori_loop(jnp.where(i == 0, 1, 0), 8, send, 0)

    def step(s, _):
        for lag, stage in zip(STAGES, (gather, relay, compute, add_far, give_back)):
            if stage is compute:

                @pl.when(s == lag)
                def _():
                    for load in loads[:3]:
                        load.wait()

            @pl.when(jnp.logical_and(s >= lag, s < lag + GROUPS))
            def _():
                stage(s - lag)

        @pl.when(s == 0)
        def _():
            gates(conv_ref, slow_ref, shift_ref, wr_ref, wi_ref, saved_ref, drive_ref, reset_ref, norm_ref, inp_ref)

        @pl.when(s == 1)
        def _():
            run_forward(first_ref, saved_ref, drive_ref, prev_ref, state_ref)

        @pl.when(s == 2)
        def _():
            factors(
                conv_ref, gate_in_ref, slow_ref, saved_ref, merged_ref, prev_ref, state_ref, reset_ref,
                norm_ref, inp_ref,
            )

        return 0

    lax.fori_loop(0, GROUPS + STAGES[-1], step, 0)

    over_rows = ((0,), (0,))

    def weight_grads(k, _):
        cols = pl.ds(pl.multiple_of(k * 512, 512), 512)
        both_ref[cols, :] = dot(rows_ref[:, cols], grad_ref[...], over_rows).astype(BF16)
        down_ref[:, cols] = dot(hidden_ref[...], cot_ref[:, cols], over_rows).astype(BF16)
        return 0

    lax.fori_loop(0, rows_ref.shape[1] // 512, weight_grads, 0)
    stores = [
        pltpu.make_async_copy(both_ref, both_hbm, store_sem.at[0]),
        pltpu.make_async_copy(down_ref, down_hbm, store_sem.at[1]),
    ]
    for store in stores:
        store.start()

    (main, tail), low = slot_tests(code_ref[...], n_sp)
    main_pick = jnp.where(main[0] | main[1], 1.0, 0.0).astype(BF16)
    in_tail = tail[0] | tail[1]
    low_pick = jnp.where(in_tail & low, 1.0, 0.0).astype(BF16)
    high_pick = jnp.where(in_tail & ~low, 1.0, 0.0).astype(BF16)
    ret_ref[sp] = back_ref[sp]
    wait_bytes(ret_ref.at[pl.ds(0, n_sp - 1)], ret_recv)
    main_rows = ret_ref[:, :, :width].astype(F32).reshape(n_sp * 8, width).astype(BF16)
    tail_rows = ret_ref[:, :, width:].astype(F32).reshape(n_sp * 8, half).astype(BF16)
    summed = dot(main_pick, main_rows, over_rows) + jnp.concatenate(
        [dot(low_pick, tail_rows, over_rows), dot(high_pick, tail_rows, over_rows)], axis=1
    )
    mix_ref[tp] = (d_out_ref[...].astype(F32) + summed).astype(BF16)
    for k in (1, 3, 2):
        to = (tp + k) % n_tp
        remote(mix_ref.at[tp], mix_ref.at[tp], mix_send.at[k - 1], mix_recv.at[k - 1], sp, to).start()
    loads[3].wait()

    slot_of = (0, 1, 3, 2)
    for n, k in enumerate(slot_of):
        q = (tp + n_tp - k) % n_tp
        if k:
            wait_bytes(mix_ref.at[q], mix_recv.at[k - 1])
        whole = mix_ref[q]
        block = dot(whole, wo_ref[:, pl.ds(pl.multiple_of(q * width, width), width)], ((1,), (1,)))
        if n == 0:
            acc_ref[...] = block
        else:
            acc_ref[...] += block
        for h in (0, 1):
            slot = 2 * n + h
            grad = dot(whole[:, h * half : (h + 1) * half], merged_ref[...], over_rows)
            grad = grad.reshape(4, 2, half // 8, width)
            keep_ref[slot] = jnp.where(c == 0, grad[:, 0], grad[:, 1])
            pair_ref[slot] = jnp.where(c == 0, grad[:, 1], grad[:, 0]).astype(BF16)
            remote(
                pair_ref.at[slot], pair_got.at[slot], pair_send, pair_recv.at[slot], sp + 1 - 2 * c, tp
            ).start()

    d_merged = acc_ref[...]
    gate_ref[...] = (d_merged * saved_ref[5]).astype(BF16)
    acc_ref[...] = d_merged * saved_ref[6]

    def back(group, carry):
        for i in range(8):
            t = pl.ds(tokens - 1 - (group * 8 + i), 1)
            grad = acc_ref[t, :] + carry
            local_ref[t, :] = grad
            carry = grad * saved_ref[0, t, :]
        return carry

    lead = lax.fori_loop(0, tokens // 8, back, jnp.zeros((1, width), F32))
    lead_ref[0, 0:1, :] = saved_ref[1, 0:1, :] * saved_ref[0, 0:1, :]
    lead_ref[0, 1:2, :] = lead
    lead_got[sp] = lead_ref[0]

    def tell(k, _):
        remote(lead_ref.at[0], lead_got.at[sp], lead_send, lead_recv, (sp + k) % n_sp, tp).start()
        return 0

    lax.fori_loop(1, n_sp, tell, 0)

    for slot in range(8):
        wait_bytes(pair_got.at[slot], pair_recv.at[slot])
        total = keep_ref[slot] + pair_got[slot].astype(F32)
        keep_ref[slot] = total
        x_ref[slot] = total.astype(BF16)
        for dx in (1, 3, 2):
            to = (x + dx) % 4
            remote(
                x_ref.at[slot, to], x_got.at[slot, dx - 1], x_send, x_recv.at[slot],
                z * 8 + to * 2 + c, tp,
            ).start()

    for slot in range(8):
        wait_bytes(x_got.at[slot], x_recv.at[slot])
        total = keep_ref[slot, x] + x_got[slot, 0].astype(F32) + x_got[slot, 1].astype(F32) + x_got[slot, 2].astype(F32)
        z_ref[slot] = total.astype(BF16)
        to = 2 * ((tp + n_tp - slot_of[slot // 2]) % n_tp) + slot % 2

        @pl.when(to == z)
        def _():
            own_ref[...] = total

        @pl.when(to != z)
        def _():
            remote(z_ref.at[slot], z_got.at[z], z_send, z_recv, to * 8 + x * 2 + c, tp).start()

    wait_bytes(lead_got.at[pl.ds(0, n_sp - 1)], lead_recv)

    def later(k, carry):
        i = n_sp - 1 - k
        pair = lead_got[i]
        return jnp.where(i > sp, pair[1:2, :] + pair[0:1, :] * carry, carry)

    incoming = lax.fori_loop(0, n_sp, later, jnp.zeros((1, width), F32))
    heads, hd = wr_ref.shape[0], wr_ref.shape[1]
    for h in range(heads):
        cols = slice(h * hd, (h + 1) * hd)
        grad = local_ref[:, cols] + saved_ref[1, :, cols] * incoming[:, cols]
        by_reset = (grad * saved_ref[2, :, cols]).astype(BF16)
        by_input = (grad * saved_ref[3, :, cols]).astype(BF16)
        rec_ref[:, cols] = (
            grad * saved_ref[4, :, cols]
            + dot(by_reset, wr_ref[h], ((1,), (1,)))
            + dot(by_input, wi_ref[h], ((1,), (1,)))
        ).astype(BF16)

    wait_bytes(z_got.at[pl.ds(0, 7)], z_recv)
    total = own_ref[...]
    for d in range(1, 8):
        total = total + z_got[(z + d) % 8].astype(F32)
    proj_ref[...] = total

    wait_bytes(send_ref.at[pl.ds(0, n_sp - 1)], send_sem)
    for side in (0, 1):
        wait_bytes(got_ref.at[tp], y_send.at[side])
        wait_bytes(got_ref.at[tp, pl.ds(0, n_sp // 2)], f_send.at[side])
        wait_bytes(part_ref.at[tp, pl.ds(0, n_sp // 2)], far_send.at[side])
        wait_bytes(part_ref.at[tp], near_send.at[side])
    for k in range(n_tp - 1):
        wait_bytes(mix_ref.at[tp], mix_send.at[k])
    wait_bytes(back_ref.at[pl.ds(0, n_sp - 1)], ret_send)
    wait_bytes(pair_ref, pair_send)
    wait_bytes(x_ref.at[:, pl.ds(0, 3)], x_send)
    wait_bytes(z_ref.at[pl.ds(0, 7)], z_send)
    wait_bytes(lead_got.at[pl.ds(0, n_sp - 1)], lead_send)
    for store in stores:
        store.wait()


def whole_step(n_sp, n_tp, *args):
    conv, w_gate = args[0], args[12]
    tokens, width = conv.shape
    model, fe = w_gate.shape
    packed = width + width // 2
    rows = n_sp * 12
    block = (model // n_sp, width)
    dma = pltpu.SemaphoreType.DMA
    specs = [VM] * 15
    for k in (7, 12, 13, 14):
        specs[k] = ANY
    return pl.pallas_call(
        step_kernel,
        out_shape=(
            jax.ShapeDtypeStruct((model, 2 * fe), BF16),
            jax.ShapeDtypeStruct((fe, model), BF16),
            jax.ShapeDtypeStruct(block, F32),
            jax.ShapeDtypeStruct((tokens, width), BF16),
            jax.ShapeDtypeStruct((tokens, width), BF16),
        ),
        in_specs=specs,
        out_specs=(ANY, ANY, VM, VM, VM),
        scratch_shapes=[
            pltpu.VMEM((n_sp, 16, packed), BF16),
            pltpu.VMEM((2, tokens), jnp.int32),
            pltpu.VMEM((n_tp, n_sp, 16, packed), BF16),
            pltpu.VMEM((rows, model), BF16),
            pltpu.VMEM((rows, model), BF16),
            pltpu.VMEM((rows, 2 * fe), BF16),
            pltpu.VMEM((rows, fe), BF16),
            pltpu.VMEM((n_tp, n_sp, 8, packed), BF16),
            pltpu.VMEM((2, GROUPS, 4, 8, packed), BF16),
            pltpu.VMEM((2, GROUPS, 4, 8, packed), BF16),
            pltpu.VMEM((2, GROUPS, 8, 8, packed), BF16),
            pltpu.VMEM((n_sp, 8, packed), BF16),
            pltpu.VMEM((n_sp, 8, packed), BF16),
            pltpu.VMEM((7, tokens, width), F32),
            pltpu.VMEM((tokens, width), BF16),
            pltpu.VMEM((6, tokens, width), F32),
            pltpu.VMEM((model, 2 * fe), BF16),
            pltpu.VMEM((fe, model), BF16),
            pltpu.VMEM((width, model), BF16),
            pltpu.VMEM((model, 2 * fe), BF16),
            pltpu.VMEM((fe, model), BF16),
            pltpu.VMEM((n_tp, tokens, width), BF16),
            pltpu.VMEM((tokens, width), F32),
            pltpu.VMEM((tokens, width), F32),
            pltpu.VMEM((8, 4, *block), F32),
            pltpu.VMEM((8, 4, *block), BF16),
            pltpu.VMEM((8, 4, *block), BF16),
            pltpu.VMEM((8, 4, *block), BF16),
            pltpu.VMEM((8, 3, *block), BF16),
            pltpu.VMEM((8, *block), BF16),
            pltpu.VMEM((8, *block), BF16),
            pltpu.VMEM(block, F32),
            pltpu.VMEM((1, 2, width), F32),
            pltpu.VMEM((n_sp, 2, width), F32),
            dma((4,)), dma((2,)), dma, dma((8,)), dma((2,)), dma((2, 8)), dma((2,)), dma((2, 8)),
            dma((2,)), dma((2, 8)), dma((2,)), dma((2, 8)), dma, dma, dma((3,)), dma((3,)),
            dma, dma((8,)), dma, dma((8,)), dma, dma, dma, dma,
        ],
        compiler_params=pltpu.CompilerParams(
            collective_id=0, has_side_effects=True, vmem_limit_bytes=63 * 2**20
        ),
        name="whole_step",
    )(*args)


def write_kernel(both_ref, down_ref, proj_ref, rec_ref, gate_ref, gg_ref, gu_ref, gd_ref, p_ref, r_ref, g_ref):
    fe = gg_ref.shape[1]
    gg_ref[...] = both_ref[:, :fe].astype(F32)
    gu_ref[...] = both_ref[:, fe:].astype(F32)
    gd_ref[...] = down_ref[...].astype(F32)
    p_ref[...] = proj_ref[...]
    r_ref[...] = rec_ref[...]
    g_ref[...] = gate_ref[...]


def write_out(both, down, proj, rec, gate, parts=4):
    model, fe = both.shape[0], both.shape[1] // 2

    def cut(array):
        return pl.BlockSpec((array.shape[0] // parts, array.shape[1]), lambda i: (i, 0))

    outs = (
        jax.ShapeDtypeStruct((model, fe), F32),
        jax.ShapeDtypeStruct((model, fe), F32),
        jax.ShapeDtypeStruct((fe, model), F32),
        jax.ShapeDtypeStruct(proj.shape, proj.dtype),
        jax.ShapeDtypeStruct(rec.shape, rec.dtype),
        jax.ShapeDtypeStruct(gate.shape, gate.dtype),
    )
    ins = (both, down, proj, rec, gate)
    return pl.pallas_call(
        write_kernel,
        grid=(parts,),
        out_shape=outs,
        in_specs=[cut(a) for a in ins],
        out_specs=tuple(cut(a) for a in outs),
        name="write_out",
    )(*ins)


def body(
    n_sp, n_tp, conv_out, gate_in, block_states, decay_param, decay_shift, w_reset, w_input, w_out,
    mixed, d_out, expert_ids, route_weights, w_gate, w_up, w_down,
):
    slow = jax.nn.softplus(-decay_param)[None, :]
    both, down, proj, rec, gate = whole_step(
        n_sp, n_tp, conv_out, gate_in, block_states, slow, decay_shift[None, :], w_reset, w_input, w_out,
        mixed, d_out, expert_ids.T, route_weights.T, w_gate[0], w_up[0], w_down[0],
    )
    gg, gu, gd, proj, rec, gate = write_out(both, down, proj, rec, gate)
    return gg[None], gu[None], gd[None], proj, rec, gate


def solution(mesh):
    in_specs = (
        P("sp", "tp"), P("sp", "tp"), P("sp", "tp"), P("tp"), P("sp"),
        P("tp", None, None), P("tp", None, None), P("tp", None),
        P("sp", "tp"), P("sp", "tp"), P("sp", None), P("sp", None),
        P("sp", None, "tp"), P("sp", None, "tp"), P("sp", "tp", None),
    )
    out_specs = (
        P("sp", None, "tp"), P("sp", None, "tp"), P("sp", "tp", None),
        P("sp", "tp"), P("sp", "tp"), P("sp", "tp"),
    )
    run = functools.partial(body, mesh.shape["sp"], mesh.shape["tp"])
    return jax.shard_map(run, mesh=mesh, in_specs=in_specs, out_specs=out_specs, check_vma=False)
```

time: 199 us -> 155 us (0.78)
  Pallas kernels: 192 us -> 153 us
  local copies, waits for them, and re-layouts: 5.49 us -> 0 us
    pallas_call x5 -> x2, Pallas kernels: 192 us -> 153 us  [the longest x1 147 us: whole_step(): pl.pallas_call(step_kernel, out_shape=(jax.ShapeDtypeStruct((model, 2 * f...]
    unnamed x7 -> x0, local copies, waits for them, and re-layouts: 4.72 us -> none
where the time goes in v2:
time: 155 us; the launch traced here: 154 us
  Pallas kernels  153 us (99%)
    pallas_call x1, Pallas kernels, whole_step(): pl.pallas_call(step_kernel, out_shape=(jax.ShapeDtypeStruct((model, 2 * f...  147 us
    pallas_call x1, Pallas kernels, write_out(): pl.pallas_call(write_kernel, grid=(parts,), out_shape=outs, in_specs=[cut...  5.23 us

profile of v2, /device:TPU:16, one launch (start us, length us, event | category | flops | bytes accessed | tf_op | source)
XLA Modules:
  0.0 154.5 jit_solution(13361581866288519938)
XLA Ops:
  0.6 1.3 compare_select_fusion
  1.9 147.3 %whole_step.1 = (bf16[2048,512]{1,0:T(8,128)(2,1)}, bf16[256,2048]{1,0:T(8,128)(2,1)}, f32[32,512]{1,0:T(8,128)}, bf16[192,512]{1,0:T(8,128)(2,1)}, bf16[192,512]{1,0:T(8,128)(2,1)}) custom-call(bf16[192,512]{1,0:T(8,128)(2,1)} %conv_ref.1, bf16[192,512]{1,0:T(8,128)(2,1)} %gate_in_ref.1, f32[1,512]{1,0:T(1,128)} %first_ref.1, f32[1,512]{1,0:T(1,128)} %bitcast.13, ...), custom_call_target="tpu_custom_call" | custom-call | tf_op jit(solution)/shard_map/whole_step/pallas_call | solution.py:551
  149.2 5.2 %write_out.1 = (f32[2048,256]{1,0:T(8,128)}, f32[2048,256]{1,0:T(8,128)}, f32[256,2048]{1,0:T(8,128)}, f32[32,512]{1,0:T(8,128)}, bf16[192,512]{1,0:T(8,128)(2,1)}, /*index=5*/bf16[192,512]{1,0:T(8,128)(2,1)}) custom-call(bf16[2048,512]{1,0:T(8,128)(2,1)} %get-tuple-element.17.both_ref, bf16[256,2048]{1,0:T(8,128)(2,1)} %get-tuple-element.18.down_ref, ...), custom_call_target="tpu_custom_call" | custom-call | tf_op jit(solution)/shard_map/write_out/pallas_call | solution.py:633

commit v3 on v2

--- a/solution.py
+++ b/solution.py
@@ -26,10 +26,12 @@
     return lax.broadcasted_iota(jnp.int32, shape, 1) < 4
 
 
-def gates(conv_ref, slow_ref, shift_ref, wr_ref, wi_ref, saved_ref, drive_ref, reset_ref, norm_ref, inp_ref):
+def gates(conv_ref, param_ref, slow_ref, shift_ref, wr_ref, wi_ref, saved_ref, drive_ref, reset_ref, norm_ref, inp_ref):
     hd = wr_ref.shape[1]
     rows = conv_ref.shape[0]
     shift = jnp.transpose(jnp.broadcast_to(shift_ref[...], (8, rows)))[:, 0:1]
+    param = param_ref[...]
+    slow_ref[...] = jnp.maximum(-param, 0.0) + jnp.log1p(jnp.exp(-jnp.abs(param)))
     for h in range(wr_ref.shape[0]):
         cols = slice(h * hd, (h + 1) * hd)
         conv = conv_ref[:, cols]
@@ -156,8 +158,11 @@
     return sp, tp, sp // 8, (sp // 2) % 4, sp % 2
 
 
+Z_ORDER = (0, 1, 6, 2, 5, 4, 3, 7)
+
+
 def z_offset(i):
-    return ((i % 2) * ((i + 1) // 2) + (1 - i % 2) * (8 - i // 2)) % 8
+    return sum(jnp.where(i == k, dz, 0) for k, dz in enumerate(Z_ORDER))
 
 
 def offset_device(z, x, c, dz, j):
@@ -226,7 +231,7 @@
 def row_part(q, at, row, grad_ref, wboth_ref, part_ref):
     packed = part_ref.shape[3]
     width, half = packed * 2 // 3, packed // 3
-    part = dot(grad_ref[pl.ds(row, 96), :], wboth_ref[q * width : (q + 1) * width, :], ((1,), (1,)))
+    part = dot(grad_ref[pl.ds(row, 96), :], wboth_ref[pl.ds(pl.multiple_of(q * width, width), width), :], ((1,), (1,)))
     part_ref[q, pl.ds(at, 8), :, :width] = part[:64].reshape(8, 8, width).astype(BF16)
     tails = part[64:].reshape(4, 8, width)
     left, right = tails[:, :, :half], tails[:, :, half:]
@@ -241,14 +246,14 @@
 
 
 def step_kernel(
-    conv_ref, gate_in_ref, first_ref, slow_ref, shift_ref, wr_ref, wi_ref, wo_hbm, mixed_ref, d_out_ref,
+    conv_ref, gate_in_ref, first_ref, param_ref, shift_ref, wr_ref, wi_ref, wo_hbm, mixed_ref, d_out_ref,
     ids_ref, wts_ref, wg_hbm, wu_hbm, wd_hbm,
     both_hbm, down_hbm, proj_ref, rec_ref, gate_ref,
     send_ref, code_ref, got_ref, rows_ref, cot_ref, grad_ref, hidden_ref, part_ref, far_ref, comb_ref,
-    near_ref, back_ref, ret_ref, saved_ref, merged_ref, temp_ref, wboth_ref, wd_ref, wo_ref, both_ref,
-    down_ref, mix_ref, acc_ref, local_ref, keep_ref, pair_ref, pair_got, x_ref, x_got, z_ref, z_got,
+    near_ref, back_ref, ret_ref, saved_ref, merged_ref, temp_ref, slow_ref, wboth_ref, wd_ref, wo_ref, both_ref,
+    down_ref, mix_ref, acc_ref, local_ref, keep_ref, pair_ref, pair_got, x_ref, x_far_ref, x_comb_ref, x_near_ref, z_ref, z_got,
     own_ref, lead_ref, lead_got,
-    load_sem, store_sem, send_sem, recv_sem, y_send, y_recv, f_send, f_recv, far_send, far_recv,
+    load_sem, store_sem, send_sem, near_x_recv, recv_sem, y_send, y_recv, f_send, f_recv, far_send, far_recv,
     near_send, near_recv, ret_send, ret_recv, mix_send, mix_recv, pair_send, pair_recv,
     x_send, x_recv, z_send, z_recv, lead_send, lead_recv,
 ):
@@ -272,36 +277,52 @@
         load.start()
     pack(ids_ref, wts_ref, d_out_ref, mixed_ref, send_ref, code_ref)
     got_ref[tp, sp] = send_ref[sp]
+    gates(
+        conv_ref, param_ref, slow_ref, shift_ref, wr_ref, wi_ref, saved_ref, drive_ref, reset_ref, norm_ref, inp_ref
+    )
+    run_forward(first_ref, saved_ref, drive_ref, prev_ref, state_ref)
+    factors(
+        conv_ref, gate_in_ref, slow_ref, saved_ref, merged_ref, prev_ref, state_ref, reset_ref, norm_ref, inp_ref
+    )
     all_here(n_sp, n_tp)
 
-    def send_group(i, _):
-        def send(j, _):
-            to = offset_device(z, x, c, z_offset(i), j)
-            remote(send_ref.at[to], got_ref.at[tp, sp], send_sem, recv_sem.at[i], to, tp).start()
-            return 0
-
-        lax.fori_loop(jnp.where(i == 0, 1, 0), 8, send, 0)
-        return 0
-
-    lax.fori_loop(0, GROUPS, send_group, 0)
+    for dx in (0, 1, 3, 2):
+        for dc in (0, 1):
+            if dx or dc:
+                to = z * 8 + ((x + dx) % 4) * 2 + (c + dc) % 2
+                remote(send_ref.at[to], got_ref.at[tp, sp], send_sem, near_x_recv.at[dx], to, tp).start()
+
+    def gather_block(i, at, count):
+        block = got_ref.at[tp, pl.ds(at, count)]
+        remote(block, block, y_send.at[0], y_recv.at[0, i], sp, right).start()
+        remote(block, block, y_send.at[1], y_recv.at[1, i], sp, left).start()
+
+    for dx in (0, 1, 3, 2):
+        at = z * 8 + ((x + 4 - dx) % 4) * 2
+        wait_bytes(got_ref.at[tp, pl.ds(at, 2 if dx else 1)], near_x_recv.at[dx])
+        gather_block(0, at, 2)
+        if dx == 0:
+
+            def send_group(i, _):
+                def send(j, _):
+                    to = offset_device(z, x, c, z_offset(i), j)
+                    remote(send_ref.at[to], got_ref.at[tp, sp], send_sem, recv_sem.at[i], to, tp).start()
+                    return 0
+
+                lax.fori_loop(0, 8, send, 0)
+                return 0
+
+            lax.fori_loop(1, GROUPS, send_group, 0)
 
     def source_group(i):
         return (z + 8 - z_offset(i)) % 8
 
     def gather(i):
-        at = source_group(i) * 8
-
-        @pl.when(i == 0)
-        def _():
-            wait_bytes(got_ref.at[tp, pl.ds(at, 7)], recv_sem.at[i])
-
         @pl.when(i > 0)
         def _():
+            at = source_group(i) * 8
             wait_bytes(got_ref.at[tp, pl.ds(at, 8)], recv_sem.at[i])
-
-        block = got_ref.at[tp, pl.ds(at, 8)]
-        remote(block, block, y_send.at[0], y_recv.at[0, i], sp, right).start()
-        remote(block, block, y_send.at[1], y_recv.at[1, i], sp, left).start()
+            gather_block(i, at, 8)
 
     def relay(i):
         at = source_group(i) * 8
@@ -320,17 +341,19 @@
         for q in range(n_tp):
             unpack(got_ref, q, at, row, rows_ref, cot_ref)
         expert_terms(row, rows_ref, cot_ref, grad_ref, hidden_ref, wboth_ref, wd_ref)
-        for q in range(n_tp):
-            row_part(q, at, row, grad_ref, wboth_ref, part_ref)
         lower, upper = pl.ds(at, 4), pl.ds(at + 4, 4)
+        row_part(far, at, row, grad_ref, wboth_ref, part_ref)
         remote(part_ref.at[far, lower], far_ref.at[0, i], far_send.at[0], far_recv.at[0, i], sp, left).start()
         remote(part_ref.at[far, upper], far_ref.at[1, i], far_send.at[1], far_recv.at[1, i], sp, right).start()
+        row_part(left, at, row, grad_ref, wboth_ref, part_ref)
         remote(
             part_ref.at[left, upper], near_ref.at[0, i, pl.ds(4, 4)], near_send.at[0], near_recv.at[0, i], sp, left
         ).start()
+        row_part(right, at, row, grad_ref, wboth_ref, part_ref)
         remote(
             part_ref.at[right, lower], near_ref.at[1, i, pl.ds(0, 4)], near_send.at[1], near_recv.at[1, i], sp, right
         ).start()
+        row_part(tp, at, row, grad_ref, wboth_ref, part_ref)
 
     def add_far(i):
         at = source_group(i) * 8
@@ -370,21 +393,6 @@
             @pl.when(jnp.logical_and(s >= lag, s < lag + GROUPS))
             def _():
                 stage(s - lag)
-
-        @pl.when(s == 0)
-        def _():
-            gates(conv_ref, slow_ref, shift_ref, wr_ref, wi_ref, saved_ref, drive_ref, reset_ref, norm_ref, inp_ref)
-
-        @pl.when(s == 1)
-        def _():
-            run_forward(first_ref, saved_ref, drive_ref, prev_ref, state_ref)
-
-        @pl.when(s == 2)
-        def _():
-            factors(
-                conv_ref, gate_in_ref, slow_ref, saved_ref, merged_ref, prev_ref, state_ref, reset_ref,
-                norm_ref, inp_ref,
-            )
 
         return 0
 
@@ -419,16 +427,20 @@
         [dot(low_pick, tail_rows, over_rows), dot(high_pick, tail_rows, over_rows)], axis=1
     )
     mix_ref[tp] = (d_out_ref[...].astype(F32) + summed).astype(BF16)
-    for k in (1, 3, 2):
-        to = (tp + k) % n_tp
-        remote(mix_ref.at[tp], mix_ref.at[tp], mix_send.at[k - 1], mix_recv.at[k - 1], sp, to).start()
+    for side, to in enumerate((right, left)):
+        remote(mix_ref.at[tp], mix_ref.at[tp], mix_send.at[side], mix_recv.at[side], sp, to).start()
     loads[3].wait()
 
-    slot_of = (0, 1, 3, 2)
-    for n, k in enumerate(slot_of):
-        q = (tp + n_tp - k) % n_tp
-        if k:
-            wait_bytes(mix_ref.at[q], mix_recv.at[k - 1])
+    blocks = (tp, left, right, far)
+    x_right, x_left, x_far = (x + 1) % 4, (x + 3) % 4, (x + 2) % 4
+    part_rows = half // 8
+    cut = part_rows // 2
+
+    def along(x_to, z_to=z):
+        return z_to * 8 + x_to * 2 + c
+
+    def products(n):
+        q = blocks[n]
         whole = mix_ref[q]
         block = dot(whole, wo_ref[:, pl.ds(pl.multiple_of(q * width, width), width)], ((1,), (1,)))
         if n == 0:
@@ -438,12 +450,76 @@
         for h in (0, 1):
             slot = 2 * n + h
             grad = dot(whole[:, h * half : (h + 1) * half], merged_ref[...], over_rows)
-            grad = grad.reshape(4, 2, half // 8, width)
+            grad = grad.reshape(4, 2, part_rows, width)
             keep_ref[slot] = jnp.where(c == 0, grad[:, 0], grad[:, 1])
             pair_ref[slot] = jnp.where(c == 0, grad[:, 1], grad[:, 0]).astype(BF16)
             remote(
                 pair_ref.at[slot], pair_got.at[slot], pair_send, pair_recv.at[slot], sp + 1 - 2 * c, tp
             ).start()
+
+    def x_start(n):
+        for slot in (2 * n, 2 * n + 1):
+            wait_bytes(pair_got.at[slot], pair_recv.at[slot])
+            total = keep_ref[slot] + pair_got[slot].astype(F32)
+            keep_ref[slot] = total
+            x_ref[slot] = total.astype(BF16)
+            lower, upper = pl.ds(0, cut), pl.ds(cut, cut)
+            for block, rows, ref, side, at, to in (
+                (x_far, lower, x_far_ref, 0, None, x_left),
+                (x_far, upper, x_far_ref, 1, None, x_right),
+                (x_left, upper, x_near_ref, 0, upper, x_left),
+                (x_right, lower, x_near_ref, 1, lower, x_right),
+            ):
+                goal = ref.at[slot, side] if at is None else ref.at[slot, side, at]
+                send, recv = (x_send.at[0], x_recv.at[0, slot, side]) if at is None else (x_send.at[1], x_recv.at[1, slot, side])
+                remote(x_ref.at[slot, block, rows], goal, send, recv, along(to), tp).start()
+
+    def x_relay(n):
+        for slot in (2 * n, 2 * n + 1):
+            for side, to, first in ((0, x_left, 0), (1, x_right, cut)):
+                wait_bytes(x_far_ref.at[slot, side], x_recv.at[0, slot, side])
+                own = keep_ref[slot, to, first : first + cut]
+                x_comb_ref[slot, side] = (own + x_far_ref[slot, side].astype(F32)).astype(BF16)
+                remote(
+                    x_comb_ref.at[slot, side], x_near_ref.at[slot, side, pl.ds(first, cut)],
+                    x_send.at[1], x_recv.at[1, slot, side], along(to), tp,
+                ).start()
+
+    def z_start(n):
+        for h in (0, 1):
+            slot = 2 * n + h
+            total = keep_ref[slot, x]
+            for side in (0, 1):
+                wait_bytes(x_near_ref.at[slot, side], x_recv.at[1, slot, side])
+                total = total + x_near_ref[slot, side].astype(F32)
+            z_ref[slot] = total.astype(BF16)
+            to = 2 * blocks[n] + h
+
+            @pl.when(to == z)
+            def _():
+                own_ref[...] = total
+
+            @pl.when(to != z)
+            def _():
+                remote(z_ref.at[slot], z_got.at[z], z_send, z_recv, along(x, to), tp).start()
+
+    upper_half = tokens // 2
+    products(0)
+    wait_bytes(mix_ref.at[left], mix_recv.at[0])
+    piece = mix_ref.at[left, pl.ds(0, upper_half)]
+    remote(piece, piece, mix_send.at[2], mix_recv.at[2], sp, right).start()
+    wait_bytes(mix_ref.at[right], mix_recv.at[1])
+    piece = mix_ref.at[right, pl.ds(upper_half, upper_half)]
+    remote(piece, piece, mix_send.at[3], mix_recv.at[3], sp, left).start()
+    x_start(0)
+    products(1)
+    products(2)
+    x_start(1)
+    x_relay(0)
+    x_start(2)
+    wait_bytes(mix_ref.at[far, pl.ds(0, upper_half)], mix_recv.at[2])
+    wait_bytes(mix_ref.at[far, pl.ds(upper_half, upper_half)], mix_recv.at[3])
+    products(3)
 
     d_merged = acc_ref[...]
     gate_ref[...] = (d_merged * saved_ref[5]).astype(BF16)
@@ -461,38 +537,19 @@
     lead_ref[0, 0:1, :] = saved_ref[1, 0:1, :] * saved_ref[0, 0:1, :]
     lead_ref[0, 1:2, :] = lead
     lead_got[sp] = lead_ref[0]
+    x_start(3)
 
     def tell(k, _):
         remote(lead_ref.at[0], lead_got.at[sp], lead_send, lead_recv, (sp + k) % n_sp, tp).start()
         return 0
 
     lax.fori_loop(1, n_sp, tell, 0)
-
-    for slot in range(8):
-        wait_bytes(pair_got.at[slot], pair_recv.at[slot])
-        total = keep_ref[slot] + pair_got[slot].astype(F32)
-        keep_ref[slot] = total
-        x_ref[slot] = total.astype(BF16)
-        for dx in (1, 3, 2):
-            to = (x + dx) % 4
-            remote(
-                x_ref.at[slot, to], x_got.at[slot, dx - 1], x_send, x_recv.at[slot],
-                z * 8 + to * 2 + c, tp,
-            ).start()
-
-    for slot in range(8):
-        wait_bytes(x_got.at[slot], x_recv.at[slot])
-        total = keep_ref[slot, x] + x_got[slot, 0].astype(F32) + x_got[slot, 1].astype(F32) + x_got[slot, 2].astype(F32)
-        z_ref[slot] = total.astype(BF16)
-        to = 2 * ((tp + n_tp - slot_of[slot // 2]) % n_tp) + slot % 2
-
-        @pl.when(to == z)
-        def _():
-            own_ref[...] = total
-
-        @pl.when(to != z)
-        def _():
-            remote(z_ref.at[slot], z_got.at[z], z_send, z_recv, to * 8 + x * 2 + c, tp).start()
+    x_relay(1)
+    x_relay(2)
+    z_start(0)
+    x_relay(3)
+    for n in (1, 2, 3):
+        z_start(n)
 
     wait_bytes(lead_got.at[pl.ds(0, n_sp - 1)], lead_recv)
 
@@ -526,11 +583,12 @@
         wait_bytes(got_ref.at[tp, pl.ds(0, n_sp // 2)], f_send.at[side])
         wait_bytes(part_ref.at[tp, pl.ds(0, n_sp // 2)], far_send.at[side])
         wait_bytes(part_ref.at[tp], near_send.at[side])
-    for k in range(n_tp - 1):
-        wait_bytes(mix_ref.at[tp], mix_send.at[k])
+        wait_bytes(mix_ref.at[tp], mix_send.at[side])
+        wait_bytes(mix_ref.at[tp, pl.ds(0, upper_half)], mix_send.at[2 + side])
     wait_bytes(back_ref.at[pl.ds(0, n_sp - 1)], ret_send)
     wait_bytes(pair_ref, pair_send)
-    wait_bytes(x_ref.at[:, pl.ds(0, 3)], x_send)
+    wait_bytes(x_far_ref, x_send.at[0])
+    wait_bytes(x_near_ref, x_send.at[1])
     wait_bytes(z_ref.at[pl.ds(0, 7)], z_send)
     wait_bytes(lead_got.at[pl.ds(0, n_sp - 1)], lead_send)
     for store in stores:
@@ -576,6 +634,7 @@
             pltpu.VMEM((7, tokens, width), F32),
             pltpu.VMEM((tokens, width), BF16),
             pltpu.VMEM((6, tokens, width), F32),
+            pltpu.VMEM((1, width), F32),
             pltpu.VMEM((model, 2 * fe), BF16),
             pltpu.VMEM((fe, model), BF16),
             pltpu.VMEM((width, model), BF16),
@@ -588,15 +647,17 @@
             pltpu.VMEM((8, 4, *block), BF16),
             pltpu.VMEM((8, 4, *block), BF16),
             pltpu.VMEM((8, 4, *block), BF16),
-            pltpu.VMEM((8, 3, *block), BF16),
+            pltpu.VMEM((8, 2, block[0] // 2, width), BF16),
+            pltpu.VMEM((8, 2, block[0] // 2, width), BF16),
+            pltpu.VMEM((8, 2, *block), BF16),
             pltpu.VMEM((8, *block), BF16),
             pltpu.VMEM((8, *block), BF16),
             pltpu.VMEM(block, F32),
             pltpu.VMEM((1, 2, width), F32),
             pltpu.VMEM((n_sp, 2, width), F32),
-            dma((4,)), dma((2,)), dma, dma((8,)), dma((2,)), dma((2, 8)), dma((2,)), dma((2, 8)),
-            dma((2,)), dma((2, 8)), dma((2,)), dma((2, 8)), dma, dma, dma((3,)), dma((3,)),
-            dma, dma((8,)), dma, dma((8,)), dma, dma, dma, dma,
+            dma((4,)), dma((2,)), dma, dma((4,)), dma((8,)), dma((2,)), dma((2, 8)), dma((2,)), dma((2, 8)),
+            dma((2,)), dma((2, 8)), dma((2,)), dma((2, 8)), dma, dma, dma((4,)), dma((4,)),
+            dma, dma((8,)), dma((2,)), dma((2, 8, 2)), dma, dma, dma, dma,
         ],
         compiler_params=pltpu.CompilerParams(
             collective_id=0, has_side_effects=True, vmem_limit_bytes=63 * 2**20
@@ -644,9 +705,8 @@
     n_sp, n_tp, conv_out, gate_in, block_states, decay_param, decay_shift, w_reset, w_input, w_out,
     mixed, d_out, expert_ids, route_weights, w_gate, w_up, w_down,
 ):
-    slow = jax.nn.softplus(-decay_param)[None, :]
     both, down, proj, rec, gate = whole_step(
-        n_sp, n_tp, conv_out, gate_in, block_states, slow, decay_shift[None, :], w_reset, w_input, w_out,
+        n_sp, n_tp, conv_out, gate_in, block_states, decay_param[None, :], decay_shift[None, :], w_reset, w_input, w_out,
         mixed, d_out, expert_ids.T, route_weights.T, w_gate[0], w_up[0], w_down[0],
     )
     gg, gu, gd, proj, rec, gate = write_out(both, down, proj, rec, gate)

time: 155 us -> 142 us (0.916)
  Pallas kernels: 153 us -> 141 us
    pallas_call x1, Pallas kernels: 147 us -> 136 us  [whole_step(): pl.pallas_call(step_kernel, out_shape=(jax.ShapeDtypeStruct((model, 2 * f...]
where the time goes in v3:
time: 142 us
  Pallas kernels  141 us (99%)
    pallas_call x1, Pallas kernels, whole_step(): pl.pallas_call(step_kernel, out_shape=(jax.ShapeDtypeStruct((model, 2 * f...  136 us
    pallas_call x1, Pallas kernels, write_out(): pl.pallas_call(write_kernel, grid=(parts,), out_shape=outs, in_specs=[cut...  5.23 us

profile of v3, /device:TPU:16, one launch (start us, length us, event | category | flops | bytes accessed | tf_op | source)
XLA Modules:
  0.0 142.1 jit_solution(16635360157867754123)
XLA Ops:
  0.6 136.2 %whole_step.1 = (bf16[2048,512]{1,0:T(8,128)(2,1)}, bf16[256,2048]{1,0:T(8,128)(2,1)}, f32[32,512]{1,0:T(8,128)}, bf16[192,512]{1,0:T(8,128)(2,1)}, bf16[192,512]{1,0:T(8,128)(2,1)}) custom-call(bf16[192,512]{1,0:T(8,128)(2,1)} %conv_ref.1, bf16[192,512]{1,0:T(8,128)(2,1)} %gate_in_ref.1, f32[1,512]{1,0:T(1,128)} %first_ref.1, f32[1,512]{1,0:T(1,128)} %bitcast.13, ...), custom_call_target="tpu_custom_call" | custom-call | tf_op jit(solution)/shard_map/whole_step/pallas_call | solution.py:609
  136.9 5.2 %write_out.1 = (f32[2048,256]{1,0:T(8,128)}, f32[2048,256]{1,0:T(8,128)}, f32[256,2048]{1,0:T(8,128)}, f32[32,512]{1,0:T(8,128)}, bf16[192,512]{1,0:T(8,128)(2,1)}, /*index=5*/bf16[192,512]{1,0:T(8,128)(2,1)}) custom-call(bf16[2048,512]{1,0:T(8,128)(2,1)} %get-tuple-element.17.both_ref, bf16[256,2048]{1,0:T(8,128)(2,1)} %get-tuple-element.18.down_ref, ...), custom_call_target="tpu_custom_call" | custom-call | tf_op jit(solution)/shard_map/write_out/pallas_call | solution.py:694

commit v4 on v3

--- a/solution.py
+++ b/solution.py
@@ -173,10 +173,12 @@
     barrier = pltpu.get_barrier_semaphore()
 
     def to_sp(k, _):
-        pl.semaphore_signal(barrier, inc=1, device_id=((sp + k) % n_sp, tp), device_id_type=MESH)
+        to = (sp + n_sp // 2 + k) % n_sp
+        pl.semaphore_signal(barrier, inc=1, device_id=(to, tp), device_id_type=MESH)
         return 0
 
-    lax.fori_loop(1, n_sp, to_sp, 0)
+    lax.fori_loop(0, n_sp // 2, to_sp, 0)
+    lax.fori_loop(1 - n_sp // 2, 0, to_sp, 0)
     for k in range(1, n_tp):
         pl.semaphore_signal(barrier, inc=1, device_id=(sp, (tp + k) % n_tp), device_id_type=MESH)
 
@@ -241,21 +243,21 @@
     part_ref[q, pl.ds(at, 8), :, width:] = jnp.stack([one, two], axis=1).reshape(8, 8, half).astype(BF16)
 
 
-STAGES = (0, 2, 3, 4, 5)
 GROUPS = 8
 
 
 def step_kernel(
-    conv_ref, gate_in_ref, first_ref, param_ref, shift_ref, wr_ref, wi_ref, wo_hbm, mixed_ref, d_out_ref,
-    ids_ref, wts_ref, wg_hbm, wu_hbm, wd_hbm,
+    conv_hbm, gate_in_hbm, first_hbm, param_hbm, shift_hbm, wr_hbm, wi_hbm, wo_hbm, mixed_hbm, d_out_hbm,
+    ids_hbm, wts_hbm, wg_hbm, wu_hbm, wd_hbm,
     both_hbm, down_hbm, proj_ref, rec_ref, gate_ref,
+    conv_ref, gate_in_ref, first_ref, param_ref, shift_ref, wr_ref, wi_ref, mixed_ref, d_out_ref, ids_ref, wts_ref,
     send_ref, code_ref, got_ref, rows_ref, cot_ref, grad_ref, hidden_ref, part_ref, far_ref, comb_ref,
     near_ref, back_ref, ret_ref, saved_ref, merged_ref, temp_ref, slow_ref, wboth_ref, wd_ref, wo_ref, both_ref,
     down_ref, mix_ref, acc_ref, local_ref, keep_ref, pair_ref, pair_got, x_ref, x_far_ref, x_comb_ref, x_near_ref, z_ref, z_got,
-    own_ref, lead_ref, lead_got,
-    load_sem, store_sem, send_sem, near_x_recv, recv_sem, y_send, y_recv, f_send, f_recv, far_send, far_recv,
+    own_ref, lead_ref, plane_ref, plane_got, line_got,
+    load_sem, store_sem, send_sem, recv_sem, y_send, y_recv, f_send, f_recv, far_send, far_recv,
     near_send, near_recv, ret_send, ret_recv, mix_send, mix_recv, pair_send, pair_recv,
-    x_send, x_recv, z_send, z_recv, lead_send, lead_recv,
+    x_send, x_recv, z_send, z_recv, plane_send, plane_recv, line_send, line_recv,
 ):
     sp, tp, z, x, c = place()
     n_tp, n_sp = part_ref.shape[0], part_ref.shape[1]
@@ -269,14 +271,21 @@
     loads = [
         pltpu.make_async_copy(src, dst, load_sem.at[k])
         for k, (src, dst) in enumerate((
+            (ids_hbm, ids_ref), (wts_hbm, wts_ref), (d_out_hbm, d_out_ref), (mixed_hbm, mixed_ref),
+            (conv_hbm, conv_ref), (param_hbm, param_ref), (shift_hbm, shift_ref), (wr_hbm, wr_ref), (wi_hbm, wi_ref),
+            (first_hbm, first_ref), (gate_in_hbm, gate_in_ref),
             (wg_hbm, wboth_ref.at[:, pl.ds(0, fe)]), (wu_hbm, wboth_ref.at[:, pl.ds(fe, fe)]),
             (wd_hbm, wd_ref), (wo_hbm, wo_ref),
         ))
     ]
     for load in loads:
         load.start()
+    for load in loads[:4]:
+        load.wait()
     pack(ids_ref, wts_ref, d_out_ref, mixed_ref, send_ref, code_ref)
     got_ref[tp, sp] = send_ref[sp]
+    for load in loads[4:11]:
+        load.wait()
     gates(
         conv_ref, param_ref, slow_ref, shift_ref, wr_ref, wi_ref, saved_ref, drive_ref, reset_ref, norm_ref, inp_ref
     )
@@ -286,43 +295,37 @@
     )
     all_here(n_sp, n_tp)
 
-    for dx in (0, 1, 3, 2):
+    x_order = (0, 1, 3, 2)
+    for dx in x_order:
         for dc in (0, 1):
             if dx or dc:
                 to = z * 8 + ((x + dx) % 4) * 2 + (c + dc) % 2
-                remote(send_ref.at[to], got_ref.at[tp, sp], send_sem, near_x_recv.at[dx], to, tp).start()
-
-    def gather_block(i, at, count):
-        block = got_ref.at[tp, pl.ds(at, count)]
+                remote(send_ref.at[to], got_ref.at[tp, sp], send_sem, recv_sem.at[0, dx], to, tp).start()
+
+    def send_group(i, _):
+        for dx in x_order:
+            for dc in (0, 1):
+                to = offset_device(z, x, c, z_offset(i), 2 * dx + dc)
+                remote(send_ref.at[to], got_ref.at[tp, sp], send_sem, recv_sem.at[i, dx], to, tp).start()
+        return 0
+
+    def source_group(i):
+        return (z + 8 - z_offset(i)) % 8
+
+    def gather_pair(i, dx):
+        at = source_group(i) * 8 + ((x + 4 - dx) % 4) * 2
+        wait_bytes(got_ref.at[tp, pl.ds(at, 1 if isinstance(i, int) and i + dx == 0 else 2)], recv_sem.at[i, dx])
+        block = got_ref.at[tp, pl.ds(at, 2)]
         remote(block, block, y_send.at[0], y_recv.at[0, i], sp, right).start()
         remote(block, block, y_send.at[1], y_recv.at[1, i], sp, left).start()
 
-    for dx in (0, 1, 3, 2):
-        at = z * 8 + ((x + 4 - dx) % 4) * 2
-        wait_bytes(got_ref.at[tp, pl.ds(at, 2 if dx else 1)], near_x_recv.at[dx])
-        gather_block(0, at, 2)
-        if dx == 0:
-
-            def send_group(i, _):
-                def send(j, _):
-                    to = offset_device(z, x, c, z_offset(i), j)
-                    remote(send_ref.at[to], got_ref.at[tp, sp], send_sem, recv_sem.at[i], to, tp).start()
-                    return 0
-
-                lax.fori_loop(0, 8, send, 0)
-                return 0
-
-            lax.fori_loop(1, GROUPS, send_group, 0)
-
-    def source_group(i):
-        return (z + 8 - z_offset(i)) % 8
-
     def gather(i):
-        @pl.when(i > 0)
+        @pl.when(i > 1)
         def _():
-            at = source_group(i) * 8
-            wait_bytes(got_ref.at[tp, pl.ds(at, 8)], recv_sem.at[i])
-            gather_block(i, at, 8)
+            gather_pair(i, 0)
+
+        for dx in x_order[1:]:
+            gather_pair(i, dx)
 
     def relay(i):
         at = source_group(i) * 8
@@ -341,19 +344,20 @@
         for q in range(n_tp):
             unpack(got_ref, q, at, row, rows_ref, cot_ref)
         expert_terms(row, rows_ref, cot_ref, grad_ref, hidden_ref, wboth_ref, wd_ref)
+        for q in range(n_tp):
+            row_part(q, at, row, grad_ref, wboth_ref, part_ref)
+
+    def reduce(i):
+        at = source_group(i) * 8
         lower, upper = pl.ds(at, 4), pl.ds(at + 4, 4)
-        row_part(far, at, row, grad_ref, wboth_ref, part_ref)
         remote(part_ref.at[far, lower], far_ref.at[0, i], far_send.at[0], far_recv.at[0, i], sp, left).start()
         remote(part_ref.at[far, upper], far_ref.at[1, i], far_send.at[1], far_recv.at[1, i], sp, right).start()
-        row_part(left, at, row, grad_ref, wboth_ref, part_ref)
         remote(
             part_ref.at[left, upper], near_ref.at[0, i, pl.ds(4, 4)], near_send.at[0], near_recv.at[0, i], sp, left
         ).start()
-        row_part(right, at, row, grad_ref, wboth_ref, part_ref)
         remote(
             part_ref.at[right, lower], near_ref.at[1, i, pl.ds(0, 4)], near_send.at[1], near_recv.at[1, i], sp, right
         ).start()
-        row_part(tp, at, row, grad_ref, wboth_ref, part_ref)
 
     def add_far(i):
         at = source_group(i) * 8
@@ -381,22 +385,35 @@
 
         lax.fori_loop(jnp.where(i == 0, 1, 0), 8, send, 0)
 
+    gather_pair(0, 0)
+    lax.fori_loop(1, GROUPS, send_group, 0)
+    gather_pair(0, 1)
+    gather_pair(0, 3)
+    gather_pair(1, 0)
+    gather_pair(0, 2)
+
+    stages = (
+        (reduce, 5, 0, 5), (gather, 0, 1, 7), (relay, 1, 0, 8), (compute, 2, 0, 8), (add_far, 6, 0, 4),
+        (give_back, 7, 0, 3),
+    )
+
     def step(s, _):
-        for lag, stage in zip(STAGES, (gather, relay, compute, add_far, give_back)):
+        for stage, begin, group, count in stages:
             if stage is compute:
 
-                @pl.when(s == lag)
+                @pl.when(s == begin)
                 def _():
-                    for load in loads[:3]:
+                    for load in loads[11:14]:
                         load.wait()
 
-            @pl.when(jnp.logical_and(s >= lag, s < lag + GROUPS))
+            @pl.when(jnp.logical_and(s >= begin, s < begin + count))
             def _():
-                stage(s - lag)
+                stage(s - begin + group)
 
         return 0
 
-    lax.fori_loop(0, GROUPS + STAGES[-1], step, 0)
+    lax.fori_loop(0, 10, step, 0)
+    lax.fori_loop(5, GROUPS, lambda i, _: reduce(i) or 0, 0)
 
     over_rows = ((0,), (0,))
 
@@ -414,11 +431,19 @@
     for store in stores:
         store.start()
 
+    def finish_rows(i, _):
+        add_far(i)
+        give_back(i - 1)
+        return 0
+
+    lax.fori_loop(4, GROUPS, finish_rows, 0)
+
     (main, tail), low = slot_tests(code_ref[...], n_sp)
     main_pick = jnp.where(main[0] | main[1], 1.0, 0.0).astype(BF16)
     in_tail = tail[0] | tail[1]
     low_pick = jnp.where(in_tail & low, 1.0, 0.0).astype(BF16)
     high_pick = jnp.where(in_tail & ~low, 1.0, 0.0).astype(BF16)
+    give_back(GROUPS - 1)
     ret_ref[sp] = back_ref[sp]
     wait_bytes(ret_ref.at[pl.ds(0, n_sp - 1)], ret_recv)
     main_rows = ret_ref[:, :, :width].astype(F32).reshape(n_sp * 8, width).astype(BF16)
@@ -429,7 +454,7 @@
     mix_ref[tp] = (d_out_ref[...].astype(F32) + summed).astype(BF16)
     for side, to in enumerate((right, left)):
         remote(mix_ref.at[tp], mix_ref.at[tp], mix_send.at[side], mix_recv.at[side], sp, to).start()
-    loads[3].wait()
+    loads[14].wait()
 
     blocks = (tp, left, right, far)
     x_right, x_left, x_far = (x + 1) % 4, (x + 3) % 4, (x + 2) % 4
@@ -505,13 +530,13 @@
 
     upper_half = tokens // 2
     products(0)
+    x_start(0)
     wait_bytes(mix_ref.at[left], mix_recv.at[0])
     piece = mix_ref.at[left, pl.ds(0, upper_half)]
     remote(piece, piece, mix_send.at[2], mix_recv.at[2], sp, right).start()
     wait_bytes(mix_ref.at[right], mix_recv.at[1])
     piece = mix_ref.at[right, pl.ds(upper_half, upper_half)]
     remote(piece, piece, mix_send.at[3], mix_recv.at[3], sp, left).start()
-    x_start(0)
     products(1)
     products(2)
     x_start(1)
@@ -536,29 +561,41 @@
     lead = lax.fori_loop(0, tokens // 8, back, jnp.zeros((1, width), F32))
     lead_ref[0, 0:1, :] = saved_ref[1, 0:1, :] * saved_ref[0, 0:1, :]
     lead_ref[0, 1:2, :] = lead
-    lead_got[sp] = lead_ref[0]
+    own_at = sp % 8
+    plane_got[own_at] = lead_ref[0]
+    for dx in (2, 1, 3, 0):
+        for dc in (1, 0):
+            if dx or dc:
+                to = z * 8 + ((x + dx) % 4) * 2 + (c + dc) % 2
+                remote(lead_ref.at[0], plane_got.at[own_at], plane_send, plane_recv, to, tp).start()
     x_start(3)
-
-    def tell(k, _):
-        remote(lead_ref.at[0], lead_got.at[sp], lead_send, lead_recv, (sp + k) % n_sp, tp).start()
-        return 0
-
-    lax.fori_loop(1, n_sp, tell, 0)
     x_relay(1)
     x_relay(2)
+
+    wait_bytes(plane_got.at[pl.ds(0, 7)], plane_recv)
+    prod, carry = jnp.ones((1, width), F32), jnp.zeros((1, width), F32)
+    own_prod, own_carry = prod, carry
+    for k in range(7, -1, -1):
+        own_prod, own_carry = jnp.where(k == own_at, prod, own_prod), jnp.where(k == own_at, carry, own_carry)
+        pair = plane_got[k]
+        carry = pair[1:2, :] + pair[0:1, :] * carry
+        prod = pair[0:1, :] * prod
+    plane_ref[0, 0:1, :] = prod
+    plane_ref[0, 1:2, :] = carry
+    line_got[z] = plane_ref[0]
+    for dz in (4, 3, 5, 2, 6, 1, 7):
+        remote(plane_ref.at[0], line_got.at[z], line_send, line_recv, along(x, (z + dz) % 8), tp).start()
     z_start(0)
     x_relay(3)
     for n in (1, 2, 3):
         z_start(n)
 
-    wait_bytes(lead_got.at[pl.ds(0, n_sp - 1)], lead_recv)
-
-    def later(k, carry):
-        i = n_sp - 1 - k
-        pair = lead_got[i]
-        return jnp.where(i > sp, pair[1:2, :] + pair[0:1, :] * carry, carry)
-
-    incoming = lax.fori_loop(0, n_sp, later, jnp.zeros((1, width), F32))
+    wait_bytes(line_got.at[pl.ds(0, 7)], line_recv)
+    carry = jnp.zeros((1, width), F32)
+    for k in range(7, 0, -1):
+        pair = line_got[k]
+        carry = jnp.where(k > z, pair[1:2, :] + pair[0:1, :] * carry, carry)
+    incoming = own_carry + own_prod * carry
     heads, hd = wr_ref.shape[0], wr_ref.shape[1]
     for h in range(heads):
         cols = slice(h * hd, (h + 1) * hd)
@@ -590,7 +627,8 @@
     wait_bytes(x_far_ref, x_send.at[0])
     wait_bytes(x_near_ref, x_send.at[1])
     wait_bytes(z_ref.at[pl.ds(0, 7)], z_send)
-    wait_bytes(lead_got.at[pl.ds(0, n_sp - 1)], lead_send)
+    wait_bytes(plane_got.at[pl.ds(0, 7)], plane_send)
+    wait_bytes(line_got.at[pl.ds(0, 7)], line_send)
     for store in stores:
         store.wait()
 
@@ -603,9 +641,7 @@
     rows = n_sp * 12
     block = (model // n_sp, width)
     dma = pltpu.SemaphoreType.DMA
-    specs = [VM] * 15
-    for k in (7, 12, 13, 14):
-        specs[k] = ANY
+    inner = (0, 1, 2, 3, 4, 5, 6, 8, 9, 10, 11)
     return pl.pallas_call(
         step_kernel,
         out_shape=(
@@ -615,9 +651,10 @@
             jax.ShapeDtypeStruct((tokens, width), BF16),
             jax.ShapeDtypeStruct((tokens, width), BF16),
         ),
-        in_specs=specs,
+        in_specs=[ANY] * 15,
         out_specs=(ANY, ANY, VM, VM, VM),
         scratch_shapes=[
+            *(pltpu.VMEM(args[k].shape, args[k].dtype) for k in inner),
             pltpu.VMEM((n_sp, 16, packed), BF16),
             pltpu.VMEM((2, tokens), jnp.int32),
             pltpu.VMEM((n_tp, n_sp, 16, packed), BF16),
@@ -654,10 +691,12 @@
             pltpu.VMEM((8, *block), BF16),
             pltpu.VMEM(block, F32),
             pltpu.VMEM((1, 2, width), F32),
-            pltpu.VMEM((n_sp, 2, width), F32),
-            dma((4,)), dma((2,)), dma, dma((4,)), dma((8,)), dma((2,)), dma((2, 8)), dma((2,)), dma((2, 8)),
+            pltpu.VMEM((1, 2, width), F32),
+            pltpu.VMEM((8, 2, width), F32),
+            pltpu.VMEM((8, 2, width), F32),
+            dma((15,)), dma((2,)), dma, dma((8, 4)), dma((2,)), dma((2, 8)), dma((2,)), dma((2, 8)),
             dma((2,)), dma((2, 8)), dma((2,)), dma((2, 8)), dma, dma, dma((4,)), dma((4,)),
-            dma, dma((8,)), dma((2,)), dma((2, 8, 2)), dma, dma, dma, dma,
+            dma, dma((8,)), dma((2,)), dma((2, 8, 2)), dma, dma, dma, dma, dma, dma,
         ],
         compiler_params=pltpu.CompilerParams(
             collective_id=0, has_side_effects=True, vmem_limit_bytes=63 * 2**20

time: 142 us -> 144 us (1.014)
  Pallas kernels: 141 us -> 143 us
    pallas_call x1, Pallas kernels: 136 us -> 138 us  [whole_step(): pl.pallas_call(step_kernel, out_shape=(jax.ShapeDtypeStruct((model, 2 * f...]
where the time goes in v4:
time: 144 us
  Pallas kernels  143 us (99%)
    pallas_call x1, Pallas kernels, whole_step(): pl.pallas_call(step_kernel, out_shape=(jax.ShapeDtypeStruct((model, 2 * f...  138 us
    pallas_call x1, Pallas kernels, write_out(): pl.pallas_call(write_kernel, grid=(parts,), out_shape=outs, in_specs=[cut...  5.23 us

profile of v4, /device:TPU:16, one launch (start us, length us, event | category | flops | bytes accessed | tf_op | source)
XLA Modules:
  0.0 143.7 jit_solution(6282053754685438512)
XLA Ops:
  0.6 137.8 %whole_step.1 = (bf16[2048,512]{1,0:T(8,128)(2,1)}, bf16[256,2048]{1,0:T(8,128)(2,1)}, f32[32,512]{1,0:T(8,128)}, bf16[192,512]{1,0:T(8,128)(2,1)}, bf16[192,512]{1,0:T(8,128)(2,1)}) custom-call(bf16[192,512]{1,0:T(8,128)(2,1)} %conv_hbm.1, bf16[192,512]{1,0:T(8,128)(2,1)} %gate_in_hbm.1, f32[1,512]{1,0:T(1,128)} %first_hbm.1, f32[1,512]{1,0:T(1,128)} %bitcast.13, ...), custom_call_target="tpu_custom_call" | custom-call | tf_op jit(solution)/shard_map/whole_step/pallas_call | solution.py:645
  138.5 5.2 %write_out.1 = (f32[2048,256]{1,0:T(8,128)}, f32[2048,256]{1,0:T(8,128)}, f32[256,2048]{1,0:T(8,128)}, f32[32,512]{1,0:T(8,128)}, bf16[192,512]{1,0:T(8,128)(2,1)}, /*index=5*/bf16[192,512]{1,0:T(8,128)(2,1)}) custom-call(bf16[2048,512]{1,0:T(8,128)(2,1)} %get-tuple-element.17.both_ref, bf16[256,2048]{1,0:T(8,128)(2,1)} %get-tuple-element.18.down_ref, ...), custom_call_target="tpu_custom_call" | custom-call | tf_op jit(solution)/shard_map/write_out/pallas_call | solution.py:733

commit v5 on v4

--- a/solution.py
+++ b/solution.py
@@ -158,11 +158,18 @@
     return sp, tp, sp // 8, (sp // 2) % 4, sp % 2
 
 
-Z_ORDER = (0, 1, 6, 2, 5, 4, 3, 7)
+Z_ORDER = (0, 1, 6, 3, 5, 4, 2, 7)
+
+
+WORK_ORDER = (2, 3, 4, 5, 6, 1, 7, 0)
 
 
 def z_offset(i):
     return sum(jnp.where(i == k, dz, 0) for k, dz in enumerate(Z_ORDER))
+
+
+def work_order(i):
+    return sum(jnp.where(i == k, group, 0) for k, group in enumerate(WORK_ORDER))
 
 
 def offset_device(z, x, c, dz, j):
@@ -249,9 +256,9 @@
 def step_kernel(
     conv_hbm, gate_in_hbm, first_hbm, param_hbm, shift_hbm, wr_hbm, wi_hbm, wo_hbm, mixed_hbm, d_out_hbm,
     ids_hbm, wts_hbm, wg_hbm, wu_hbm, wd_hbm,
-    both_hbm, down_hbm, proj_ref, rec_ref, gate_ref,
+    both_hbm, down_hbm, proj_hbm, rec_hbm, gate_hbm,
     conv_ref, gate_in_ref, first_ref, param_ref, shift_ref, wr_ref, wi_ref, mixed_ref, d_out_ref, ids_ref, wts_ref,
-    send_ref, code_ref, got_ref, rows_ref, cot_ref, grad_ref, hidden_ref, part_ref, far_ref, comb_ref,
+    proj_ref, rec_ref, gate_ref, send_ref, code_ref, got_ref, rows_ref, cot_ref, grad_ref, hidden_ref, part_ref, far_ref, comb_ref,
     near_ref, back_ref, ret_ref, saved_ref, merged_ref, temp_ref, slow_ref, wboth_ref, wd_ref, wo_ref, both_ref,
     down_ref, mix_ref, acc_ref, local_ref, keep_ref, pair_ref, pair_got, x_ref, x_far_ref, x_comb_ref, x_near_ref, z_ref, z_got,
     own_ref, lead_ref, plane_ref, plane_got, line_got,
@@ -393,8 +400,8 @@
     gather_pair(0, 2)
 
     stages = (
-        (reduce, 5, 0, 5), (gather, 0, 1, 7), (relay, 1, 0, 8), (compute, 2, 0, 8), (add_far, 6, 0, 4),
-        (give_back, 7, 0, 3),
+        (compute, 4, 0, 8), (add_far, 6, 0, 8), (give_back, 7, 0, 8), (reduce, 4, 0, 8), (gather, 0, 1, 7),
+        (relay, 0, 0, 8),
     )
 
     def step(s, _):
@@ -408,12 +415,12 @@
 
             @pl.when(jnp.logical_and(s >= begin, s < begin + count))
             def _():
-                stage(s - begin + group)
+                number = s - begin + group
+                stage(number if stage in (gather, relay) else work_order(number))
 
         return 0
 
-    lax.fori_loop(0, 10, step, 0)
-    lax.fori_loop(5, GROUPS, lambda i, _: reduce(i) or 0, 0)
+    lax.fori_loop(0, GROUPS + 7, step, 0)
 
     over_rows = ((0,), (0,))
 
@@ -427,23 +434,18 @@
     stores = [
         pltpu.make_async_copy(both_ref, both_hbm, store_sem.at[0]),
         pltpu.make_async_copy(down_ref, down_hbm, store_sem.at[1]),
+        pltpu.make_async_copy(gate_ref, gate_hbm, store_sem.at[2]),
+        pltpu.make_async_copy(rec_ref, rec_hbm, store_sem.at[3]),
+        pltpu.make_async_copy(proj_ref, proj_hbm, store_sem.at[4]),
     ]
-    for store in stores:
+    for store in stores[:2]:
         store.start()
-
-    def finish_rows(i, _):
-        add_far(i)
-        give_back(i - 1)
-        return 0
-
-    lax.fori_loop(4, GROUPS, finish_rows, 0)
 
     (main, tail), low = slot_tests(code_ref[...], n_sp)
     main_pick = jnp.where(main[0] | main[1], 1.0, 0.0).astype(BF16)
     in_tail = tail[0] | tail[1]
     low_pick = jnp.where(in_tail & low, 1.0, 0.0).astype(BF16)
     high_pick = jnp.where(in_tail & ~low, 1.0, 0.0).astype(BF16)
-    give_back(GROUPS - 1)
     ret_ref[sp] = back_ref[sp]
     wait_bytes(ret_ref.at[pl.ds(0, n_sp - 1)], ret_recv)
     main_rows = ret_ref[:, :, :width].astype(F32).reshape(n_sp * 8, width).astype(BF16)
@@ -451,9 +453,13 @@
     summed = dot(main_pick, main_rows, over_rows) + jnp.concatenate(
         [dot(low_pick, tail_rows, over_rows), dot(high_pick, tail_rows, over_rows)], axis=1
     )
-    mix_ref[tp] = (d_out_ref[...].astype(F32) + summed).astype(BF16)
-    for side, to in enumerate((right, left)):
-        remote(mix_ref.at[tp], mix_ref.at[tp], mix_send.at[side], mix_recv.at[side], sp, to).start()
+    mixed_rows = (d_out_ref[...].astype(F32) + summed).astype(BF16)
+    for h in (0, 1):
+        mix_ref[tp, h] = mixed_rows[:, h * half : (h + 1) * half]
+    for order in (0, 1):
+        for side, to in enumerate((right, left)):
+            piece = mix_ref.at[tp, (order + side) % 2]
+            remote(piece, piece, mix_send.at[side], mix_recv.at[side, order], sp, to).start()
     loads[14].wait()
 
     blocks = (tp, left, right, far)
@@ -464,26 +470,24 @@
     def along(x_to, z_to=z):
         return z_to * 8 + x_to * 2 + c
 
-    def products(n):
-        q = blocks[n]
-        whole = mix_ref[q]
-        block = dot(whole, wo_ref[:, pl.ds(pl.multiple_of(q * width, width), width)], ((1,), (1,)))
-        if n == 0:
+    def products(n, h):
+        q, slot = blocks[n], 2 * n + h
+        part = mix_ref[q, h]
+        columns = pl.ds(pl.multiple_of(q * width + h * half, half), half)
+        block = dot(part, wo_ref[:, columns], ((1,), (1,)))
+        if slot == 0:
             acc_ref[...] = block
         else:
             acc_ref[...] += block
-        for h in (0, 1):
-            slot = 2 * n + h
-            grad = dot(whole[:, h * half : (h + 1) * half], merged_ref[...], over_rows)
-            grad = grad.reshape(4, 2, part_rows, width)
-            keep_ref[slot] = jnp.where(c == 0, grad[:, 0], grad[:, 1])
-            pair_ref[slot] = jnp.where(c == 0, grad[:, 1], grad[:, 0]).astype(BF16)
-            remote(
-                pair_ref.at[slot], pair_got.at[slot], pair_send, pair_recv.at[slot], sp + 1 - 2 * c, tp
-            ).start()
-
-    def x_start(n):
-        for slot in (2 * n, 2 * n + 1):
+        grad = dot(part, merged_ref[...], over_rows).reshape(4, 2, part_rows, width)
+        keep_ref[slot] = jnp.where(c == 0, grad[:, 0], grad[:, 1])
+        pair_ref[slot] = jnp.where(c == 0, grad[:, 1], grad[:, 0]).astype(BF16)
+        remote(
+            pair_ref.at[slot], pair_got.at[slot], pair_send, pair_recv.at[slot], sp + 1 - 2 * c, tp
+        ).start()
+
+    def x_start(*slots):
+        for slot in slots:
             wait_bytes(pair_got.at[slot], pair_recv.at[slot])
             total = keep_ref[slot] + pair_got[slot].astype(F32)
             keep_ref[slot] = total
@@ -499,8 +503,8 @@
                 send, recv = (x_send.at[0], x_recv.at[0, slot, side]) if at is None else (x_send.at[1], x_recv.at[1, slot, side])
                 remote(x_ref.at[slot, block, rows], goal, send, recv, along(to), tp).start()
 
-    def x_relay(n):
-        for slot in (2 * n, 2 * n + 1):
+    def x_relay(*slots):
+        for slot in slots:
             for side, to, first in ((0, x_left, 0), (1, x_right, cut)):
                 wait_bytes(x_far_ref.at[slot, side], x_recv.at[0, slot, side])
                 own = keep_ref[slot, to, first : first + cut]
@@ -510,15 +514,14 @@
                     x_send.at[1], x_recv.at[1, slot, side], along(to), tp,
                 ).start()
 
-    def z_start(n):
-        for h in (0, 1):
-            slot = 2 * n + h
+    def z_start(*slots):
+        for slot in slots:
             total = keep_ref[slot, x]
             for side in (0, 1):
                 wait_bytes(x_near_ref.at[slot, side], x_recv.at[1, slot, side])
                 total = total + x_near_ref[slot, side].astype(F32)
             z_ref[slot] = total.astype(BF16)
-            to = 2 * blocks[n] + h
+            to = 2 * blocks[slot // 2] + slot % 2
 
             @pl.when(to == z)
             def _():
@@ -528,26 +531,34 @@
             def _():
                 remote(z_ref.at[slot], z_got.at[z], z_send, z_recv, along(x, to), tp).start()
 
-    upper_half = tokens // 2
-    products(0)
-    x_start(0)
-    wait_bytes(mix_ref.at[left], mix_recv.at[0])
-    piece = mix_ref.at[left, pl.ds(0, upper_half)]
-    remote(piece, piece, mix_send.at[2], mix_recv.at[2], sp, right).start()
-    wait_bytes(mix_ref.at[right], mix_recv.at[1])
-    piece = mix_ref.at[right, pl.ds(upper_half, upper_half)]
-    remote(piece, piece, mix_send.at[3], mix_recv.at[3], sp, left).start()
-    products(1)
-    products(2)
-    x_start(1)
-    x_relay(0)
-    x_start(2)
-    wait_bytes(mix_ref.at[far, pl.ds(0, upper_half)], mix_recv.at[2])
-    wait_bytes(mix_ref.at[far, pl.ds(upper_half, upper_half)], mix_recv.at[3])
-    products(3)
+    def mix_arrived(side, order):
+        q, h = (left, right)[side], (order + side) % 2
+        wait_bytes(mix_ref.at[q, h], mix_recv.at[side, order])
+        if order == 0:
+            piece = mix_ref.at[q, h]
+            remote(piece, piece, mix_send.at[2 + side], mix_recv.at[2, side], sp, (right, left)[side]).start()
+
+    products(0, 0)
+    products(0, 1)
+    x_start(0, 1)
+    mix_arrived(0, 0)
+    mix_arrived(1, 0)
+    products(1, 0)
+    products(2, 1)
+    x_relay(0, 1)
+    x_start(2, 5)
+    mix_arrived(0, 1)
+    mix_arrived(1, 1)
+    products(1, 1)
+    products(2, 0)
+    x_start(3, 4)
+    for h in (0, 1):
+        wait_bytes(mix_ref.at[far, h], mix_recv.at[2, h])
+        products(3, h)
 
     d_merged = acc_ref[...]
     gate_ref[...] = (d_merged * saved_ref[5]).astype(BF16)
+    stores[2].start()
     acc_ref[...] = d_merged * saved_ref[6]
 
     def back(group, carry):
@@ -568,9 +579,10 @@
             if dx or dc:
                 to = z * 8 + ((x + dx) % 4) * 2 + (c + dc) % 2
                 remote(lead_ref.at[0], plane_got.at[own_at], plane_send, plane_recv, to, tp).start()
-    x_start(3)
-    x_relay(1)
-    x_relay(2)
+    x_relay(2, 5)
+    x_start(6, 7)
+    z_start(0, 1)
+    x_relay(3, 4)
 
     wait_bytes(plane_got.at[pl.ds(0, 7)], plane_recv)
     prod, carry = jnp.ones((1, width), F32), jnp.zeros((1, width), F32)
@@ -585,10 +597,9 @@
     line_got[z] = plane_ref[0]
     for dz in (4, 3, 5, 2, 6, 1, 7):
         remote(plane_ref.at[0], line_got.at[z], line_send, line_recv, along(x, (z + dz) % 8), tp).start()
-    z_start(0)
-    x_relay(3)
-    for n in (1, 2, 3):
-        z_start(n)
+    z_start(2, 5)
+    x_relay(6, 7)
+    z_start(3, 4, 6, 7)
 
     wait_bytes(line_got.at[pl.ds(0, 7)], line_recv)
     carry = jnp.zeros((1, width), F32)
@@ -608,11 +619,13 @@
             + dot(by_input, wi_ref[h], ((1,), (1,)))
         ).astype(BF16)
 
+    stores[3].start()
     wait_bytes(z_got.at[pl.ds(0, 7)], z_recv)
     total = own_ref[...]
     for d in range(1, 8):
         total = total + z_got[(z + d) % 8].astype(F32)
     proj_ref[...] = total
+    stores[4].start()
 
     wait_bytes(send_ref.at[pl.ds(0, n_sp - 1)], send_sem)
     for side in (0, 1):
@@ -621,7 +634,7 @@
         wait_bytes(part_ref.at[tp, pl.ds(0, n_sp // 2)], far_send.at[side])
         wait_bytes(part_ref.at[tp], near_send.at[side])
         wait_bytes(mix_ref.at[tp], mix_send.at[side])
-        wait_bytes(mix_ref.at[tp, pl.ds(0, upper_half)], mix_send.at[2 + side])
+        wait_bytes(mix_ref.at[tp, 0], mix_send.at[2 + side])
     wait_bytes(back_ref.at[pl.ds(0, n_sp - 1)], ret_send)
     wait_bytes(pair_ref, pair_send)
     wait_bytes(x_far_ref, x_send.at[0])
@@ -652,9 +665,12 @@
             jax.ShapeDtypeStruct((tokens, width), BF16),
         ),
         in_specs=[ANY] * 15,
-        out_specs=(ANY, ANY, VM, VM, VM),
+        out_specs=(ANY,) * 5,
         scratch_shapes=[
             *(pltpu.VMEM(args[k].shape, args[k].dtype) for k in inner),
+            pltpu.VMEM(block, F32),
+            pltpu.VMEM((tokens, width), BF16),
+            pltpu.VMEM((tokens, width), BF16),
             pltpu.VMEM((n_sp, 16, packed), BF16),
             pltpu.VMEM((2, tokens), jnp.int32),
             pltpu.VMEM((n_tp, n_sp, 16, packed), BF16),
@@ -677,7 +693,7 @@
             pltpu.VMEM((width, model), BF16),
             pltpu.VMEM((model, 2 * fe), BF16),
             pltpu.VMEM((fe, model), BF16),
-            pltpu.VMEM((n_tp, tokens, width), BF16),
+            pltpu.VMEM((n_tp, 2, tokens, width // 2), BF16),
             pltpu.VMEM((tokens, width), F32),
             pltpu.VMEM((tokens, width), F32),
             pltpu.VMEM((8, 4, *block), F32),
@@ -694,8 +710,8 @@
             pltpu.VMEM((1, 2, width), F32),
             pltpu.VMEM((8, 2, width), F32),
             pltpu.VMEM((8, 2, width), F32),
-            dma((15,)), dma((2,)), dma, dma((8, 4)), dma((2,)), dma((2, 8)), dma((2,)), dma((2, 8)),
-            dma((2,)), dma((2, 8)), dma((2,)), dma((2, 8)), dma, dma, dma((4,)), dma((4,)),
+            dma((15,)), dma((5,)), dma, dma((8, 4)), dma((2,)), dma((2, 8)), dma((2,)), dma((2, 8)),
+            dma((2,)), dma((2, 8)), dma((2,)), dma((2, 8)), dma, dma, dma((4,)), dma((3, 2)),
             dma, dma((8,)), dma((2,)), dma((2, 8, 2)), dma, dma, dma, dma, dma, dma,
         ],
         compiler_params=pltpu.CompilerParams(
@@ -715,7 +731,7 @@
     g_ref[...] = gate_ref[...]
 
 
-def write_out(both, down, proj, rec, gate, parts=4):
+def write_out(both, down, proj, rec, gate, parts=2):
     model, fe = both.shape[0], both.shape[1] // 2
 
     def cut(array):

time: 144 us -> 130 us (0.903)
  Pallas kernels: 143 us -> 129 us
    pallas_call x1, Pallas kernels: 138 us -> 125 us  [whole_step(): pl.pallas_call(step_kernel, out_shape=(jax.ShapeDtypeStruct((model, 2 * f...]
where the time goes in v5:
time: 130 us
  Pallas kernels  129 us (99%)
    pallas_call x1, Pallas kernels, whole_step(): pl.pallas_call(step_kernel, out_shape=(jax.ShapeDtypeStruct((model, 2 * f...  125 us
    pallas_call x1, Pallas kernels, write_out(): pl.pallas_call(write_kernel, grid=(parts,), out_shape=outs, in_specs=[cut...  4.43 us

profile of v5, /device:TPU:16, one launch (start us, length us, event | category | flops | bytes accessed | tf_op | source)
XLA Modules:
  0.0 129.8 jit_solution(13275308758050822483)
XLA Ops:
  0.6 124.7 %whole_step.1 = (bf16[2048,512]{1,0:T(8,128)(2,1)}, bf16[256,2048]{1,0:T(8,128)(2,1)}, f32[32,512]{1,0:T(8,128)}, bf16[192,512]{1,0:T(8,128)(2,1)}, bf16[192,512]{1,0:T(8,128)(2,1)}) custom-call(bf16[192,512]{1,0:T(8,128)(2,1)} %conv_hbm.1, bf16[192,512]{1,0:T(8,128)(2,1)} %gate_in_hbm.1, f32[1,512]{1,0:T(1,128)} %first_hbm.1, f32[1,512]{1,0:T(1,128)} %bitcast.13, ...), custom_call_target="tpu_custom_call" | custom-call | tf_op jit(solution)/shard_map/whole_step/pallas_call | solution.py:658
  125.3 4.4 %write_out.1 = (f32[2048,256]{1,0:T(8,128)}, f32[2048,256]{1,0:T(8,128)}, f32[256,2048]{1,0:T(8,128)}, f32[32,512]{1,0:T(8,128)}, bf16[192,512]{1,0:T(8,128)(2,1)}, /*index=5*/bf16[192,512]{1,0:T(8,128)(2,1)}) custom-call(bf16[2048,512]{1,0:T(8,128)(2,1)} %get-tuple-element.17.both_ref, bf16[256,2048]{1,0:T(8,128)(2,1)} %get-tuple-element.18.down_ref, ...), custom_call_target="tpu_custom_call" | custom-call | tf_op jit(solution)/shard_map/write_out/pallas_call | solution.py:749

commit v6 on v5

--- a/solution.py
+++ b/solution.py
@@ -100,19 +100,17 @@
         merged_ref[:, cols] = (act * state).astype(BF16)
 
 
-def slot_tests(codes, experts):
+def slot_tests(codes, experts, first=0):
     tokens = codes.shape[1]
     row = lax.broadcasted_iota(jnp.int32, (experts * 8, tokens), 0)
-    base = (row // 8) * 16
+    base = (row // 8 + first) * 16
     main = base + row % 8
     tail = base + 8 + row % 4
     return [[codes[k : k + 1, :] == want for k in (0, 1)] for want in (main, tail)], row % 8 < 4
 
 
-def pack(ids_ref, wts_ref, d_out_ref, mixed_ref, send_ref, code_ref):
-    experts = send_ref.shape[0]
-    tokens, width = d_out_ref.shape
-    half = width // 2
+def rank_codes(ids_ref, code_ref, experts):
+    tokens = ids_ref.shape[1]
     each = lax.broadcasted_iota(jnp.int32, (experts, tokens), 0)
     named = [ids_ref[k : k + 1, :] == each for k in (0, 1)]
     both = jnp.where(named[0] | named[1], 1.0, 0.0).astype(BF16)
@@ -121,13 +119,15 @@
         < lax.broadcasted_iota(jnp.int32, (tokens, tokens), 1)
     )
     count = dot(both, jnp.where(earlier, 1.0, 0.0).astype(BF16))
-    codes = []
     for k in (0, 1):
         rank = jnp.sum(jnp.where(named[k], count, 0.0), axis=0, keepdims=True)
-        codes.append(ids_ref[k : k + 1, :] * 16 + rank.astype(jnp.int32))
-        code_ref[k : k + 1, :] = codes[k]
-    codes = jnp.concatenate(codes, axis=0)
-    (main, tail), low = slot_tests(codes, experts)
+        code_ref[k : k + 1, :] = ids_ref[k : k + 1, :] * 16 + rank.astype(jnp.int32)
+
+
+def pack(code_ref, wts_ref, raw_ref, columns, experts, first, store):
+    width = raw_ref.shape[3]
+    half = width // 2
+    (main, tail), low = slot_tests(code_ref[...], experts, first)
 
     def weight(tests):
         return jnp.sum(
@@ -140,17 +140,18 @@
     in_tail = tail[0] | tail[1]
     low_pick = jnp.where(in_tail & low, 1.0, 0.0).astype(BF16)
     high_pick = jnp.where(in_tail & ~low, 1.0, 0.0).astype(BF16)
-
-    for at, (ref, w_main, w_tail) in enumerate(
-        ((d_out_ref, weight(main), weight(tail)), (mixed_ref, None, None))
-    ):
-        first = dot(main_pick, ref[...])
-        second = dot(low_pick, ref[:, :half]) + dot(high_pick, ref[:, half:])
-        if w_main is not None:
-            first, second = first * w_main, second * w_tail
-        rows = slice(at * 8, at * 8 + 8)
-        send_ref[:, rows, :width] = first.reshape(experts, 8, width).astype(BF16)
-        send_ref[:, rows, width:] = second.reshape(experts, 8, half).astype(BF16)
+    weights = (weight(main), weight(tail))
+    for q in columns:
+        for at in (0, 1):
+            rows = raw_ref[at, q]
+            block = dot(main_pick, rows)
+            ends = dot(low_pick, rows[:, :half]) + dot(high_pick, rows[:, half:])
+            if at == 0:
+                block, ends = block * weights[0], ends * weights[1]
+            both = jnp.concatenate(
+                [block.reshape(experts, 8, width), ends.reshape(experts, 8, half)], axis=2
+            ).astype(BF16)
+            store(q, slice(at * 8, at * 8 + 8), both)
 
 
 def place():
@@ -158,18 +159,17 @@
     return sp, tp, sp // 8, (sp // 2) % 4, sp % 2
 
 
-Z_ORDER = (0, 1, 6, 3, 5, 4, 2, 7)
-
-
-WORK_ORDER = (2, 3, 4, 5, 6, 1, 7, 0)
+Z_ORDER = (2, 6, 3, 4, 5, 1, 7, 0)
+FAR_GROUPS = 5
+PLAN = (
+    1, 8, 9, 2, 17, 3, 16, 24, 11, 32, 10, 4, 40, 18,
+    26, 12, 34, 19, 25, 27, 20, 42, 33, 28, 23, 35, 22, 41,
+    30, 21, 36, 29, 31, 43, 44, 38, 37, 39, 46, 45, 47,
+)
 
 
 def z_offset(i):
     return sum(jnp.where(i == k, dz, 0) for k, dz in enumerate(Z_ORDER))
-
-
-def work_order(i):
-    return sum(jnp.where(i == k, group, 0) for k, group in enumerate(WORK_ORDER))
 
 
 def offset_device(z, x, c, dz, j):
@@ -257,18 +257,18 @@
     conv_hbm, gate_in_hbm, first_hbm, param_hbm, shift_hbm, wr_hbm, wi_hbm, wo_hbm, mixed_hbm, d_out_hbm,
     ids_hbm, wts_hbm, wg_hbm, wu_hbm, wd_hbm,
     both_hbm, down_hbm, proj_hbm, rec_hbm, gate_hbm,
-    conv_ref, gate_in_ref, first_ref, param_ref, shift_ref, wr_ref, wi_ref, mixed_ref, d_out_ref, ids_ref, wts_ref,
+    conv_ref, gate_in_ref, first_ref, param_ref, shift_ref, wr_ref, wi_ref, raw_ref, near_out, ids_ref, wts_ref,
     proj_ref, rec_ref, gate_ref, send_ref, code_ref, got_ref, rows_ref, cot_ref, grad_ref, hidden_ref, part_ref, far_ref, comb_ref,
     near_ref, back_ref, ret_ref, saved_ref, merged_ref, temp_ref, slow_ref, wboth_ref, wd_ref, wo_ref, both_ref,
     down_ref, mix_ref, acc_ref, local_ref, keep_ref, pair_ref, pair_got, x_ref, x_far_ref, x_comb_ref, x_near_ref, z_ref, z_got,
     own_ref, lead_ref, plane_ref, plane_got, line_got,
-    load_sem, store_sem, send_sem, recv_sem, y_send, y_recv, f_send, f_recv, far_send, far_recv,
+    load_sem, store_sem, raw_send, raw_recv, near_g_send, send_sem, recv_sem, y_send, y_recv, f_send, f_recv, far_send, far_recv,
     near_send, near_recv, ret_send, ret_recv, mix_send, mix_recv, pair_send, pair_recv,
     x_send, x_recv, z_send, z_recv, plane_send, plane_recv, line_send, line_recv,
 ):
     sp, tp, z, x, c = place()
     n_tp, n_sp = part_ref.shape[0], part_ref.shape[1]
-    tokens, width = d_out_ref.shape
+    tokens, width = raw_ref.shape[2:]
     half = width // 2
     fe = wd_ref.shape[0]
     right, left, far = (tp + 1) % n_tp, (tp + n_tp - 1) % n_tp, (tp + 2) % n_tp
@@ -278,7 +278,7 @@
     loads = [
         pltpu.make_async_copy(src, dst, load_sem.at[k])
         for k, (src, dst) in enumerate((
-            (ids_hbm, ids_ref), (wts_hbm, wts_ref), (d_out_hbm, d_out_ref), (mixed_hbm, mixed_ref),
+            (ids_hbm, ids_ref), (wts_hbm, wts_ref), (d_out_hbm, raw_ref.at[0, tp]), (mixed_hbm, raw_ref.at[1, tp]),
             (conv_hbm, conv_ref), (param_hbm, param_ref), (shift_hbm, shift_ref), (wr_hbm, wr_ref), (wi_hbm, wi_ref),
             (first_hbm, first_ref), (gate_in_hbm, gate_in_ref),
             (wg_hbm, wboth_ref.at[:, pl.ds(0, fe)]), (wu_hbm, wboth_ref.at[:, pl.ds(fe, fe)]),
@@ -289,50 +289,81 @@
         load.start()
     for load in loads[:4]:
         load.wait()
-    pack(ids_ref, wts_ref, d_out_ref, mixed_ref, send_ref, code_ref)
+    rank_codes(ids_ref, code_ref, n_sp)
+
+    def store_all(q, rows, value):
+        send_ref[:, rows, :] = value
+
+    pack(code_ref, wts_ref, raw_ref, (tp,), n_sp, 0, store_all)
     got_ref[tp, sp] = send_ref[sp]
-    for load in loads[4:11]:
-        load.wait()
-    gates(
-        conv_ref, param_ref, slow_ref, shift_ref, wr_ref, wi_ref, saved_ref, drive_ref, reset_ref, norm_ref, inp_ref
-    )
-    run_forward(first_ref, saved_ref, drive_ref, prev_ref, state_ref)
-    factors(
-        conv_ref, gate_in_ref, slow_ref, saved_ref, merged_ref, prev_ref, state_ref, reset_ref, norm_ref, inp_ref
-    )
     all_here(n_sp, n_tp)
 
-    x_order = (0, 1, 3, 2)
-    for dx in x_order:
-        for dc in (0, 1):
-            if dx or dc:
-                to = z * 8 + ((x + dx) % 4) * 2 + (c + dc) % 2
-                remote(send_ref.at[to], got_ref.at[tp, sp], send_sem, recv_sem.at[0, dx], to, tp).start()
-
-    def send_group(i, _):
-        for dx in x_order:
-            for dc in (0, 1):
-                to = offset_device(z, x, c, z_offset(i), 2 * dx + dc)
-                remote(send_ref.at[to], got_ref.at[tp, sp], send_sem, recv_sem.at[i, dx], to, tp).start()
+    sides = (right, left)
+    for order in (0, 1):
+        for side in (0, 1):
+            piece = raw_ref.at[(order + side) % 2, tp]
+            remote(piece, piece, raw_send.at[side], raw_recv.at[side, order], sp, sides[side]).start()
+
+    def send_far(i, _):
+        def send(j, _):
+            to = offset_device(z, x, c, z_offset(i), j)
+            remote(send_ref.at[to], got_ref.at[tp, sp], send_sem, recv_sem.at[i], to, tp).start()
+            return 0
+
+        lax.fori_loop(0, 8, send, 0)
         return 0
+
+    def send_near(g, _):
+        def send(j, _):
+            to = offset_device(z, x, c, z_offset(g), j)
+            remote(send_ref.at[to], got_ref.at[tp, sp], send_sem, recv_sem.at[g], to, tp).start()
+            return 0
+
+        lax.fori_loop(jnp.where(g == GROUPS - 1, 1, 0), 8, send, 0)
+        return 0
+
+    lax.fori_loop(0, 2, send_far, 0)
 
     def source_group(i):
         return (z + 8 - z_offset(i)) % 8
 
-    def gather_pair(i, dx):
-        at = source_group(i) * 8 + ((x + 4 - dx) % 4) * 2
-        wait_bytes(got_ref.at[tp, pl.ds(at, 1 if isinstance(i, int) and i + dx == 0 else 2)], recv_sem.at[i, dx])
-        block = got_ref.at[tp, pl.ds(at, 2)]
+    def near_blocks(columns):
+        def one(g, _):
+            target = (z + z_offset(g)) % 8
+            at = g - FAR_GROUPS
+
+            def store(q, rows, value):
+                near_out[at, q, :, rows, :] = value
+
+            pack(code_ref, wts_ref, raw_ref, columns, 8, target * 8, store)
+
+            def send(j, _):
+                slot = ((x + j // 2) % 4) * 2 + (c + j % 2) % 2
+                for q in columns:
+                    remote(
+                        near_out.at[at, q, slot], got_ref.at[q, sp], near_g_send, recv_sem.at[g], target * 8 + slot, tp
+                    ).start()
+                return 0
+
+            lax.fori_loop(jnp.where(g == GROUPS - 1, 1, 0), 8, send, 0)
+            return 0
+
+        lax.fori_loop(FAR_GROUPS, GROUPS, one, 0)
+        for q in columns:
+            got_ref[q, sp] = near_out[GROUPS - 1 - FAR_GROUPS, q, sp % 8]
+
+    def raw_arrived(side, order):
+        piece = raw_ref.at[(order + side) % 2, (left, right)[side]]
+        wait_bytes(piece, raw_recv.at[side, order])
+        if order == 0:
+            remote(piece, piece, raw_send.at[2 + side], raw_recv.at[2, side], sp, sides[side]).start()
+
+    def gather(i):
+        at = source_group(i) * 8
+        block = got_ref.at[tp, pl.ds(at, 8)]
+        wait_bytes(block, recv_sem.at[i])
         remote(block, block, y_send.at[0], y_recv.at[0, i], sp, right).start()
         remote(block, block, y_send.at[1], y_recv.at[1, i], sp, left).start()
-
-    def gather(i):
-        @pl.when(i > 1)
-        def _():
-            gather_pair(i, 0)
-
-        for dx in x_order[1:]:
-            gather_pair(i, dx)
 
     def relay(i):
         at = source_group(i) * 8
@@ -346,8 +377,20 @@
     def compute(i):
         group = source_group(i)
         at, row = group * 8, pl.multiple_of(group * 96, 32)
-        wait_bytes(got_ref.at[far, pl.ds(at, 4)], f_recv.at[0, i])
-        wait_bytes(got_ref.at[far, pl.ds(at + 4, 4)], f_recv.at[1, i])
+
+        @pl.when(i < FAR_GROUPS)
+        def _():
+            wait_bytes(got_ref.at[far, pl.ds(at, 4)], f_recv.at[0, i])
+            wait_bytes(got_ref.at[far, pl.ds(at + 4, 4)], f_recv.at[1, i])
+
+        @pl.when(jnp.logical_and(i >= FAR_GROUPS, i < GROUPS - 1))
+        def _():
+            wait_bytes(got_ref.at[:, pl.ds(at, 8)], recv_sem.at[i])
+
+        @pl.when(i == GROUPS - 1)
+        def _():
+            wait_bytes(got_ref.at[:, pl.ds(at, 7)], recv_sem.at[i])
+
         for q in range(n_tp):
             unpack(got_ref, q, at, row, rows_ref, cot_ref)
         expert_terms(row, rows_ref, cot_ref, grad_ref, hidden_ref, wboth_ref, wd_ref)
@@ -390,37 +433,45 @@
             remote(back_ref.at[to], ret_ref.at[sp], ret_send, ret_recv, to, tp).start()
             return 0
 
-        lax.fori_loop(jnp.where(i == 0, 1, 0), 8, send, 0)
-
-    gather_pair(0, 0)
-    lax.fori_loop(1, GROUPS, send_group, 0)
-    gather_pair(0, 1)
-    gather_pair(0, 3)
-    gather_pair(1, 0)
-    gather_pair(0, 2)
-
-    stages = (
-        (compute, 4, 0, 8), (add_far, 6, 0, 8), (give_back, 7, 0, 8), (reduce, 4, 0, 8), (gather, 0, 1, 7),
-        (relay, 0, 0, 8),
+        lax.fori_loop(jnp.where(i == GROUPS - 1, 1, 0), 8, send, 0)
+
+    for load in loads[4:11]:
+        load.wait()
+    gates(
+        conv_ref, param_ref, slow_ref, shift_ref, wr_ref, wi_ref, saved_ref, drive_ref, reset_ref, norm_ref, inp_ref
     )
+    raw_arrived(0, 0)
+    raw_arrived(1, 0)
+    lax.fori_loop(2, 4, send_far, 0)
+    run_forward(first_ref, saved_ref, drive_ref, prev_ref, state_ref)
+    raw_arrived(0, 1)
+    raw_arrived(1, 1)
+    gather(0)
+    lax.fori_loop(4, FAR_GROUPS, send_far, 0)
+    near_blocks((left, right))
+    lax.fori_loop(FAR_GROUPS, GROUPS, send_near, 0)
+    factors(
+        conv_ref, gate_in_ref, slow_ref, saved_ref, merged_ref, prev_ref, state_ref, reset_ref, norm_ref, inp_ref
+    )
+    for k in (0, 1):
+        wait_bytes(raw_ref.at[k, far], raw_recv.at[2, k])
+    near_blocks((far,))
+    for load in loads[11:14]:
+        load.wait()
+
+    stages = (gather, relay, compute, reduce, add_far, give_back)
 
     def step(s, _):
-        for stage, begin, group, count in stages:
-            if stage is compute:
-
-                @pl.when(s == begin)
-                def _():
-                    for load in loads[11:14]:
-                        load.wait()
-
-            @pl.when(jnp.logical_and(s >= begin, s < begin + count))
+        code = sum(jnp.where(s == k, entry, 0) for k, entry in enumerate(PLAN))
+        for k, stage in enumerate(stages):
+
+            @pl.when(code // 8 == k)
             def _():
-                number = s - begin + group
-                stage(number if stage in (gather, relay) else work_order(number))
+                stage(code % 8)
 
         return 0
 
-    lax.fori_loop(0, GROUPS + 7, step, 0)
+    lax.fori_loop(0, len(PLAN), step, 0)
 
     over_rows = ((0,), (0,))
 
@@ -430,7 +481,6 @@
         down_ref[:, cols] = dot(hidden_ref[...], cot_ref[:, cols], over_rows).astype(BF16)
         return 0
 
-    lax.fori_loop(0, rows_ref.shape[1] // 512, weight_grads, 0)
     stores = [
         pltpu.make_async_copy(both_ref, both_hbm, store_sem.at[0]),
         pltpu.make_async_copy(down_ref, down_hbm, store_sem.at[1]),
@@ -438,8 +488,7 @@
         pltpu.make_async_copy(rec_ref, rec_hbm, store_sem.at[3]),
         pltpu.make_async_copy(proj_ref, proj_hbm, store_sem.at[4]),
     ]
-    for store in stores[:2]:
-        store.start()
+    lax.fori_loop(0, 1, weight_grads, 0)
 
     (main, tail), low = slot_tests(code_ref[...], n_sp)
     main_pick = jnp.where(main[0] | main[1], 1.0, 0.0).astype(BF16)
@@ -453,7 +502,7 @@
     summed = dot(main_pick, main_rows, over_rows) + jnp.concatenate(
         [dot(low_pick, tail_rows, over_rows), dot(high_pick, tail_rows, over_rows)], axis=1
     )
-    mixed_rows = (d_out_ref[...].astype(F32) + summed).astype(BF16)
+    mixed_rows = (raw_ref[0, tp].astype(F32) + summed).astype(BF16)
     for h in (0, 1):
         mix_ref[tp, h] = mixed_rows[:, h * half : (h + 1) * half]
     for order in (0, 1):
@@ -541,6 +590,9 @@
     products(0, 0)
     products(0, 1)
     x_start(0, 1)
+    lax.fori_loop(1, 4, weight_grads, 0)
+    for store in stores[:2]:
+        store.start()
     mix_arrived(0, 0)
     mix_arrived(1, 0)
     products(1, 0)
@@ -579,10 +631,11 @@
             if dx or dc:
                 to = z * 8 + ((x + dx) % 4) * 2 + (c + dc) % 2
                 remote(lead_ref.at[0], plane_got.at[own_at], plane_send, plane_recv, to, tp).start()
+    x_start(6, 7)
     x_relay(2, 5)
-    x_start(6, 7)
     z_start(0, 1)
     x_relay(3, 4)
+    x_relay(6, 7)
 
     wait_bytes(plane_got.at[pl.ds(0, 7)], plane_recv)
     prod, carry = jnp.ones((1, width), F32), jnp.zeros((1, width), F32)
@@ -597,9 +650,7 @@
     line_got[z] = plane_ref[0]
     for dz in (4, 3, 5, 2, 6, 1, 7):
         remote(plane_ref.at[0], line_got.at[z], line_send, line_recv, along(x, (z + dz) % 8), tp).start()
-    z_start(2, 5)
-    x_relay(6, 7)
-    z_start(3, 4, 6, 7)
+    z_start(2, 5, 3, 4, 6, 7)
 
     wait_bytes(line_got.at[pl.ds(0, 7)], line_recv)
     carry = jnp.zeros((1, width), F32)
@@ -628,9 +679,12 @@
     stores[4].start()
 
     wait_bytes(send_ref.at[pl.ds(0, n_sp - 1)], send_sem)
+    wait_bytes(got_ref.at[pl.ds(0, 3), pl.ds(0, 23)], near_g_send)
     for side in (0, 1):
-        wait_bytes(got_ref.at[tp], y_send.at[side])
-        wait_bytes(got_ref.at[tp, pl.ds(0, n_sp // 2)], f_send.at[side])
+        wait_bytes(raw_ref.at[:, tp], raw_send.at[side])
+        wait_bytes(raw_ref.at[0, tp], raw_send.at[2 + side])
+        wait_bytes(got_ref.at[tp, pl.ds(0, FAR_GROUPS * 8)], y_send.at[side])
+        wait_bytes(got_ref.at[tp, pl.ds(0, FAR_GROUPS * 4)], f_send.at[side])
         wait_bytes(part_ref.at[tp, pl.ds(0, n_sp // 2)], far_send.at[side])
         wait_bytes(part_ref.at[tp], near_send.at[side])
         wait_bytes(mix_ref.at[tp], mix_send.at[side])
@@ -654,7 +708,7 @@
     rows = n_sp * 12
     block = (model // n_sp, width)
     dma = pltpu.SemaphoreType.DMA
-    inner = (0, 1, 2, 3, 4, 5, 6, 8, 9, 10, 11)
+    inner, others = (0, 1, 2, 3, 4, 5, 6), (10, 11)
     return pl.pallas_call(
         step_kernel,
         out_shape=(
@@ -668,6 +722,9 @@
         out_specs=(ANY,) * 5,
         scratch_shapes=[
             *(pltpu.VMEM(args[k].shape, args[k].dtype) for k in inner),
+            pltpu.VMEM((2, n_tp, tokens, width), BF16),
+            pltpu.VMEM((3, n_tp, 8, 16, packed), BF16),
+            *(pltpu.VMEM(args[k].shape, args[k].dtype) for k in others),
             pltpu.VMEM(block, F32),
             pltpu.VMEM((tokens, width), BF16),
             pltpu.VMEM((tokens, width), BF16),
@@ -710,7 +767,7 @@
             pltpu.VMEM((1, 2, width), F32),
             pltpu.VMEM((8, 2, width), F32),
             pltpu.VMEM((8, 2, width), F32),
-            dma((15,)), dma((5,)), dma, dma((8, 4)), dma((2,)), dma((2, 8)), dma((2,)), dma((2, 8)),
+            dma((15,)), dma((5,)), dma((4,)), dma((3, 2)), dma, dma, dma((8,)), dma((2,)), dma((2, 8)), dma((2,)), dma((2, 8)),
             dma((2,)), dma((2, 8)), dma((2,)), dma((2, 8)), dma, dma, dma((4,)), dma((3, 2)),
             dma, dma((8,)), dma((2,)), dma((2, 8, 2)), dma, dma, dma, dma, dma, dma,
         ],

time: 130 us -> 130 us (level)
  no operation moved by 1% of the time
where the time goes in v6:
time: 130 us
  Pallas kernels  129 us (99%)
    pallas_call x1, Pallas kernels, whole_step(): pl.pallas_call(step_kernel, out_shape=(jax.ShapeDtypeStruct((model, 2 * f...  125 us
    pallas_call x1, Pallas kernels, write_out(): pl.pallas_call(write_kernel, grid=(parts,), out_shape=outs, in_specs=[cut...  4.43 us

profile of v6, /device:TPU:16, one launch (start us, length us, event | category | flops | bytes accessed | tf_op | source)
XLA Modules:
  0.0 129.6 jit_solution(3204163778821439474)
XLA Ops:
  0.6 124.5 %whole_step.1 = (bf16[2048,512]{1,0:T(8,128)(2,1)}, bf16[256,2048]{1,0:T(8,128)(2,1)}, f32[32,512]{1,0:T(8,128)}, bf16[192,512]{1,0:T(8,128)(2,1)}, bf16[192,512]{1,0:T(8,128)(2,1)}) custom-call(bf16[192,512]{1,0:T(8,128)(2,1)} %conv_hbm.1, bf16[192,512]{1,0:T(8,128)(2,1)} %gate_in_hbm.1, f32[1,512]{1,0:T(1,128)} %first_hbm.1, f32[1,512]{1,0:T(1,128)} %bitcast.13, ...), custom_call_target="tpu_custom_call" | custom-call | tf_op jit(solution)/shard_map/whole_step/pallas_call | solution.py:712
  125.2 4.4 %write_out.1 = (f32[2048,256]{1,0:T(8,128)}, f32[2048,256]{1,0:T(8,128)}, f32[256,2048]{1,0:T(8,128)}, f32[32,512]{1,0:T(8,128)}, bf16[192,512]{1,0:T(8,128)(2,1)}, /*index=5*/bf16[192,512]{1,0:T(8,128)(2,1)}) custom-call(bf16[2048,512]{1,0:T(8,128)(2,1)} %get-tuple-element.17.both_ref, bf16[256,2048]{1,0:T(8,128)(2,1)} %get-tuple-element.18.down_ref, ...), custom_call_target="tpu_custom_call" | custom-call | tf_op jit(solution)/shard_map/write_out/pallas_call | solution.py:806
